TPU v7x, 32 devices: a whole 2x2x4 slice. The times are simulated.
32 devices in a mesh: sp: 16 (over z, y, x), tp: 2 (over core).
Axes of the slice: x: 2, y: 2, z: 4, core: 2. Of those that a mesh axis runs over, the one named last changes fastest.
Arguments:
- resid: bfloat16 [3072, 2048], P('sp'), may hold values from -6 to 6
- query: bfloat16 [3072, 2048], P('sp', 'tp'), may hold values from -6 to 6
- key: bfloat16 [3072, 1024], P('sp', 'tp'), may hold values from -6 to 6
- value: bfloat16 [3072, 1024], P('sp', 'tp'), may hold values from -6 to 6
- q_gain: float32 [128], replicated, may hold values from 0.3 to 5, as said below
- k_gain: float32 [128], replicated, may hold values from 0.3 to 5, as said below
- out_weight: bfloat16 [2048, 2048], P('tp'), may hold values from -0.125 to 0.125
- norm_gain: float32 [2048], replicated, may hold values from 0.1 to 1.9
- gate_weight: bfloat16 [2048, 5632], P('sp', 'tp'), may hold values from -0.125 to 0.125
- up_weight: bfloat16 [2048, 5632], P('sp', 'tp'), may hold values from -0.125 to 0.125
- down_weight: bfloat16 [5632, 2048], P('tp', 'sp'), may hold values from -0.078125 to 0.078125
Outputs:
- mixed: bfloat16 [3072, 2048], P(('sp', 'tp'))
Inputs may be any that keep to these rules, and one draw needn't show every extreme that they name: `q_gain`: positive gains. `k_gain`: positive gains.
All inputs are finite; a program needn't handle non-finite values.
Results may differ from a plain program's by a relative error of at most 0.012.
The roundings to bfloat16 on the way count: a program that leaves them out, or rounds other values in their place, can miss the bound.
Values may be sent and summed in bfloat16 or wider, within the bound.
A program may use at most 128 MiB of HBM per device.

v0:
```python
import functools
import math

import jax
import jax.numpy as jnp
import numpy as np
from jax import lax
from jax.experimental import pallas as pl
from jax.experimental.pallas import tpu as pltpu
from jax.sharding import PartitionSpec as P

GRID_W = 64


EPSILON = 1e-06


def rotate(values, positions):
    dim_size = values.shape[-1]
    half_dim = dim_size // 2
    quarter = half_dim // 2
    inverse = 10000.0 ** (-jnp.arange(quarter, dtype=jnp.float32) / quarter)
    outputs = []
    for axis_pos, coords in enumerate((positions // GRID_W, positions % GRID_W)):
        angles = coords.astype(jnp.float32)[:, None] * inverse[None, :]
        cosine = jnp.cos(angles)[:, None, :]
        sine = jnp.sin(angles)[:, None, :]
        section = values[..., axis_pos * half_dim : (axis_pos + 1) * half_dim]
        first_half = section[..., :quarter]
        second_half = section[..., quarter:]
        outputs += [
            first_half * cosine - second_half * sine,
            second_half * cosine + first_half * sine,
        ]
    return jnp.concatenate(outputs, axis=-1)


def prepare(projected, gain, positions):
    values = projected.astype(jnp.float32)
    normed = values * lax.rsqrt(jnp.mean(values * values, axis=-1, keepdims=True) + EPSILON) * gain
    return rotate(normed, positions).astype(jnp.bfloat16)


def normalize(stream, gain):
    values = stream.astype(jnp.float32)
    return (
        values * lax.rsqrt(jnp.mean(values * values, axis=-1, keepdims=True) + EPSILON) * gain
    ).astype(jnp.bfloat16)


def whole_body(
    resid,
    query,
    key,
    value,
    q_gain,
    k_gain,
    out_weight,
    norm_gain,
    gate_weight,
    up_weight,
    down_weight,
):
    rows_here = query.shape[0]
    head_dim = q_gain.shape[0]
    heads_here = query.shape[1] // head_dim
    kv_here = key.shape[1] // head_dim
    group_size = heads_here // kv_here
    score_scale = head_dim ** (-0.5)
    positions = lax.axis_index("sp") * rows_here + jnp.arange(rows_here, dtype=jnp.int32)
    q_rot = prepare(query.reshape(rows_here, heads_here, head_dim), q_gain, positions)
    k_rot = prepare(key.reshape(rows_here, kv_here, head_dim), k_gain, positions)
    val_rows = value.reshape(rows_here, kv_here, head_dim)
    grouped = q_rot.reshape(rows_here, kv_here, group_size, head_dim)

    def key_block(carry, block):
        maxima, totals, accum = carry
        block_keys, block_vals = block
        scores = (
            jnp.einsum("qkgd,skd->kgqs", grouped, block_keys, preferred_element_type=jnp.float32)
            * score_scale
        )
        new_max = jnp.maximum(maxima, jnp.max(scores, axis=-1))
        shrink = jnp.exp(maxima - new_max)
        weights = jnp.exp(scores - new_max[..., None])
        totals = totals * shrink + jnp.sum(weights, axis=-1)
        accum = accum * shrink[..., None] + jnp.einsum(
            "kgqs,skd->kgqd",
            weights.astype(jnp.bfloat16),
            block_vals,
            preferred_element_type=jnp.float32,
        )
        return ((new_max, totals, accum), None)

    start_max = jnp.full((kv_here, group_size, rows_here), -1e30, jnp.float32)
    start_total = jnp.zeros((kv_here, group_size, rows_here), jnp.float32)
    start_accum = jnp.zeros((kv_here, group_size, rows_here, head_dim), jnp.float32)
    carry = (start_max, start_total, start_accum)
    key_part = lax.all_gather(k_rot, "sp", axis=0, tiled=True)
    val_part = lax.all_gather(val_rows, "sp", axis=0, tiled=True)
    length = key_part.shape[0]
    factor = 4
    span = rows_here * factor
    turns = length // span
    key_blocks = key_part.reshape(turns, span, kv_here, head_dim)
    val_blocks = val_part.reshape(turns, span, kv_here, head_dim)
    carry, _ = lax.scan(key_block, carry, (key_blocks, val_blocks))
    maxima, totals, accum = carry
    attn = (
        jnp.transpose(accum / totals[..., None], (2, 0, 1, 3))
        .reshape(rows_here, heads_here * head_dim)
        .astype(jnp.bfloat16)
    )
    share = rows_here // lax.axis_size("tp")
    my_first = lax.axis_index("tp") * share
    proj = lax.psum_scatter(
        jnp.dot(attn, out_weight, preferred_element_type=jnp.float32).astype(jnp.bfloat16),
        "tp",
        scatter_dimension=0,
        tiled=True,
    ).astype(jnp.float32)
    my_resid = lax.dynamic_slice_in_dim(resid, my_first, share, 0)
    my_stream = (my_resid.astype(jnp.float32) + proj).astype(jnp.bfloat16)
    mixer_rows = lax.all_gather(normalize(my_stream, norm_gain), "tp", axis=0, tiled=True)

    def add_rows(shard_rows):
        return jnp.dot(mixer_rows, shard_rows, preferred_element_type=jnp.float32)

    gate = add_rows(lax.all_gather(gate_weight, "sp", axis=0, tiled=True))
    up_part = add_rows(lax.all_gather(up_weight, "sp", axis=0, tiled=True))
    hidden = (jax.nn.silu(gate) * up_part).astype(jnp.bfloat16)
    down_whole = lax.all_gather(down_weight, "sp", axis=1, tiled=True)
    down = lax.psum_scatter(
        jnp.dot(hidden, down_whole, preferred_element_type=jnp.float32).astype(jnp.bfloat16),
        "tp",
        scatter_dimension=0,
        tiled=True,
    ).astype(jnp.float32)
    return (my_stream.astype(jnp.float32) + 0.5 * down).astype(jnp.bfloat16)


SPLIT = 4


def fits(n_sp, kv_here, hidden_here):
    return n_sp % SPLIT == 0 and kv_here % SPLIT == 0 and hidden_here % (64 * SPLIT) == 0


def groups_of(n_sp):
    ranks = n_sp // SPLIT
    tokens = [[part * ranks + rank for part in range(SPLIT)] for rank in range(ranks)]
    hidden = [[part * ranks + rank for rank in range(ranks)] for part in range(SPLIT)]
    return tokens, hidden


MESH = pl.DeviceIdType.MESH


def layer_kernel(
    ranks,
    head_dim,
    key_ref,
    value_ref,
    query_ref,
    k_gain_ref,
    q_gain_ref,
    freq_ref,
    gate_ref,
    up_ref,
    down_ref,
    ow_ref,
    resid_ref,
    gain_ref,
    out_ref,
    kvb,
    qb,
    asend,
    ab,
    wgu,
    wdn,
    pj,
    prv,
    nb,
    st,
    dsb,
    drv,
    ds2,
    dzb,
    acc,
    kv_ref,
    q_ref,
    gu_ref,
    local_sem,
    kvz_s, kvz_r, kvx_s, kvx_r, q_s, q_r, gz_s, gz_r, dz_s, dz_r,
    gx_s, gx_r, dx_s, dx_r, gh_s, gh_r, dh_s, dh_r,
    at_s, at_r, pj_s, pj_r, nz_s, nz_r, np_s, np_r, dp_s, dp_r, fz_s, fz_r,
):
    sp = lax.axis_index("sp")
    core = lax.axis_index("tp")
    part = sp // ranks
    rank = sp % ranks
    rows = q_ref.shape[1]
    share = rows // 2
    depth = gu_ref.shape[1]
    width = down_ref.shape[0] // SPLIT
    cols = down_ref.shape[1]
    group = q_ref.shape[2] // head_dim
    other = 1 - core
    flips = (1, 2, 3)

    def flip(e):
        x = rank % 2
        y = rank // 2
        nx = 1 - x if e % 2 else x
        ny = 1 - y if e // 2 else y
        return ny * 2 + nx

    def peer_part(dz):
        return ((part + dz) % SPLIT) * ranks + rank

    def from_part(dz):
        return (part + SPLIT - dz) % SPLIT

    def near(e):
        return part * ranks + flip(e)

    def dn_own(index):
        return down_ref.at[pl.ds(pl.multiple_of(index * width, 16), width)]

    barrier = pltpu.get_barrier_semaphore()
    for dz in range(1, SPLIT):
        pl.semaphore_signal(barrier, inc=1, device_id=(peer_part(dz), core), device_id_type=MESH)
    for e in flips:
        pl.semaphore_signal(barrier, inc=1, device_id=(near(e), core), device_id_type=MESH)
    pl.semaphore_signal(barrier, inc=1, device_id=(sp, other), device_id_type=MESH)

    lane = lax.broadcasted_iota(jnp.int32, (rows, head_dim), 1)
    spot = sp * rows + lax.broadcasted_iota(jnp.int32, (rows, head_dim), 0)
    grid_bits = GRID_W.bit_length() - 1
    coords = jnp.where(lane < head_dim // 2, spot >> grid_bits, spot & (GRID_W - 1))
    angles = coords.astype(jnp.float32) * freq_ref[...]
    first_half = (lane & (head_dim // 2 - 1)) < head_dim // 4
    cosine = jnp.cos(angles)
    sine = jnp.where(first_half, -jnp.sin(angles), jnp.sin(angles))

    def turn(ref, head, gain):
        x = ref[:, head * head_dim : (head + 1) * head_dim].astype(jnp.float32)
        x = x * lax.rsqrt(jnp.mean(x * x, axis=-1, keepdims=True) + EPSILON) * gain[...]
        quarter = head_dim // 4
        mate = jnp.where(first_half, pltpu.roll(x, head_dim - quarter, 1), pltpu.roll(x, quarter, 1))
        return (x * cosine + mate * sine).astype(jnp.bfloat16)

    for index in range(SPLIT):
        kv_ref[index, :, 0:head_dim] = turn(key_ref, index, k_gain_ref)
        kv_ref[index, :, head_dim : 2 * head_dim] = value_ref[:, index * head_dim : (index + 1) * head_dim]
    for index in range(SPLIT):
        for head in range(group):
            lanes = slice(head * head_dim, (head + 1) * head_dim)
            q_ref[index, :, lanes] = turn(query_ref, index * group + head, q_gain_ref)
    whole_lanes = width // 128 * 128
    for index in range(SPLIT):
        start = index * width // 128 * 128
        skew = index * width - start
        rests = []
        for which, ref in enumerate((gate_ref, up_ref)):
            block = ref[:, start : start + whole_lanes + 128]
            if skew:
                block = pltpu.roll(block.astype(jnp.float32), whole_lanes + 128 - skew, 1).astype(jnp.bfloat16)
            gu_ref[index, :, which * whole_lanes : (which + 1) * whole_lanes] = block[:, :whole_lanes]
            rests.append(block[:, whole_lanes:].astype(jnp.float32))
        spread = lax.broadcasted_iota(jnp.int32, rests[0].shape, 1)
        last = jnp.where(spread < width - whole_lanes, rests[0], pltpu.roll(rests[1], width - whole_lanes, 1))
        gu_ref[index, :, 2 * whole_lanes :] = last.astype(jnp.bfloat16)

    sent = []

    def send(src, dst, s_sem, r_sem, target, keep=True):
        copy = pltpu.make_async_remote_copy(
            src_ref=src, dst_ref=dst, send_sem=s_sem, recv_sem=r_sem, device_id=target, device_id_type=MESH
        )
        copy.start()
        if keep:
            sent.append(copy)
        return copy

    def landed(dst, s_sem, r_sem):
        pltpu.make_async_remote_copy(
            src_ref=dst, dst_ref=dst, send_sem=s_sem, recv_sem=r_sem, device_id=(sp, other), device_id_type=MESH
        ).wait_recv()

    def gu_at(source, first=0, count=None):
        return wgu.at[pl.ds(pl.multiple_of(source * depth + first, 16), depth if count is None else count)]

    def dn_at(source, first=0, count=None):
        return wdn.at[pl.ds(first, width if count is None else count), pl.ds(pl.multiple_of(source * cols, cols), cols)]

    locals_ = [
        pltpu.make_async_copy(kv_ref.at[part], kvb.at[part, rank], local_sem.at[0]),
        pltpu.make_async_copy(q_ref.at[part], qb.at[part], local_sem.at[1]),
        pltpu.make_async_copy(gu_ref.at[part], gu_at(sp), local_sem.at[2]),
        pltpu.make_async_copy(dn_own(part), dn_at(sp), local_sem.at[3]),
    ]
    for copy in locals_:
        copy.start()
    pad = wdn.shape[0] - width
    wdn[pl.ds(width, pad), :] = jnp.zeros((pad, wdn.shape[1]), wdn.dtype)

    pl.semaphore_wait(barrier, SPLIT - 1 + 3 + 1)

    def to_part(dz):
        return (part + dz) % SPLIT

    for dz in range(1, SPLIT):
        send(kv_ref.at[to_part(dz)], kvb.at[part, rank], kvz_s.at[dz], kvz_r.at[dz], (peer_part(dz), core))
    for e in flips:
        send(kv_ref.at[part], kvb.at[part, rank], kvx_s.at[0, e], kvx_r.at[0, e], (near(e), core))
    for dz in range(1, SPLIT):
        send(q_ref.at[to_part(dz)], qb.at[part], q_s.at[dz], q_r.at[dz], (peer_part(dz), core))
    for e in (1, 2):
        send(dn_own(part), dn_at(sp), dx_s.at[0, e], dx_r.at[0, e], (near(e), core))
    for dz in range(1, SPLIT):
        send(gu_ref.at[to_part(dz)], gu_at(sp), gz_s.at[dz], gz_r.at[dz], (peer_part(dz), core))
        send(dn_own(to_part(dz)), dn_at(sp), dz_s.at[dz], dz_r.at[dz], (peer_part(dz), core))
    for dz in range(1, SPLIT):
        slot = kvb.at[from_part(dz), rank]
        landed(slot, kvz_s.at[dz], kvz_r.at[dz])
        for e in flips:
            send(slot, slot, kvx_s.at[dz, e], kvx_r.at[dz, e], (near(e), core))
    for e in (1, 2):
        send(gu_ref.at[part], gu_at(sp), gx_s.at[0, e], gx_r.at[0, e], (near(e), core))

    def pass_on(dz):
        source = from_part(dz) * ranks + rank
        landed(gu_at(source), gz_s.at[dz], gz_r.at[dz])
        for e in (1, 2):
            send(gu_at(source), gu_at(source), gx_s.at[dz, e], gx_r.at[dz, e], (near(e), core))
        landed(dn_at(source), dz_s.at[dz], dz_r.at[dz])
        for e in (1, 2):
            send(dn_at(source), dn_at(source), dx_s.at[dz, e], dx_r.at[dz, e], (near(e), core))

    def halves(dz):
        for e in (1, 2):
            source = from_part(dz) * ranks + flip(e)
            across = (near(3 - e), core)
            landed(gu_at(source), gx_s.at[dz, e], gx_r.at[dz, e])
            half = gu_at(source, (e - 1) * depth // 2, depth // 2)
            send(half, half, gh_s.at[dz, e], gh_r.at[dz, e], across)
            landed(dn_at(source), dx_s.at[dz, e], dx_r.at[dz, e])
            half = dn_at(source, (e - 1) * width // 2, width // 2)
            send(half, half, dh_s.at[dz, e], dh_r.at[dz, e], across)

    for dz in range(SPLIT):
        for e in flips:
            landed(kvb.at[from_part(dz), flip(e)], kvx_s.at[dz, e], kvx_r.at[dz, e])
    locals_[0].wait()
    locals_[1].wait()
    for dz in range(1, SPLIT):
        landed(qb.at[from_part(dz)], q_s.at[dz], q_r.at[dz])

    factor = head_dim ** (-0.5) * math.log2(math.e)
    length = SPLIT * ranks * rows

    def attend(source, target):
        @pl.loop(0, group)
        def _(head):
            lanes = pl.ds(pl.multiple_of(head * head_dim, head_dim), head_dim)
            q = qb[source, :, lanes]
            keys = kvb[:, :, :, pl.ds(0, head_dim)].reshape(length, head_dim)
            scores = lax.dot_general(q, keys, (((1,), (1,)), ((), ())), preferred_element_type=jnp.float32)
            peak = jnp.max(scores, axis=-1, keepdims=True)
            weights = jnp.exp2((scores - peak) * factor)
            total = jnp.sum(weights, axis=-1, keepdims=True)
            vals = kvb[:, :, :, pl.ds(head_dim, head_dim)].reshape(length, head_dim)
            summed = jnp.dot(weights.astype(jnp.bfloat16), vals, preferred_element_type=jnp.float32)
            target[:, lanes] = (summed / total).astype(jnp.bfloat16)

    for dz in (1, 2, 3):
        attend(to_part(dz), asend.at[dz])
        send(asend.at[dz], ab.at[part], at_s.at[dz], at_r.at[dz], (peer_part(dz), core))
        if dz == 2:
            pass_on(1)
    attend(part, ab.at[part])
    halves(0)
    for dz in range(1, SPLIT):
        landed(ab.at[from_part(dz)], at_s.at[dz], at_r.at[dz])

    attn = jnp.concatenate([ab[index] for index in range(SPLIT)], axis=1)
    tile = 512
    for first in range(0, ow_ref.shape[1], tile):
        block = jnp.dot(attn, ow_ref[:, first : first + tile], preferred_element_type=jnp.float32)
        pj[:, :, first : first + tile] = block.astype(jnp.bfloat16).reshape(2, share, tile)
    send(pj.at[other], prv, pj_s, pj_r, (sp, other))
    pass_on(2)
    landed(prv, pj_s, pj_r)
    proj = pj[core].astype(jnp.float32) + prv[...].astype(jnp.float32)
    stream = (resid_ref[pl.ds(pl.multiple_of(core * share, 16), share)].astype(jnp.float32) + proj).astype(jnp.bfloat16)
    st[...] = stream
    wide = stream.astype(jnp.float32)
    level = lax.rsqrt(jnp.mean(wide * wide, axis=-1, keepdims=True) + EPSILON)
    nb[part, core] = (wide * level * gain_ref[...]).astype(jnp.bfloat16)
    ahead = [(part < SPLIT - 1, sp + ranks, -1), (part > 0, sp - ranks, 1)]

    def step_on(source, step, way):
        slot = nb.at[source, core]
        go, target, _ = ahead[way]

        @pl.when(go)
        def _():
            send(slot, slot, nz_s.at[way, step], nz_r.at[way, step], (target, core), keep=False)

    def present(way, step):
        source = part + ahead[way][2] * (step + 1)
        return source, (source >= 0) & (source < SPLIT)

    step_on(part, 0, 0)
    step_on(part, 0, 1)
    mine = nb.at[part, core]
    send(mine, mine, np_s.at[part], np_r.at[part], (sp, other))
    def hop(step):
        for way in (0, 1):
            source, there = present(way, step)

            @pl.when(there)
            def _():
                slot = nb.at[source, core]
                landed(slot, nz_s.at[way, step], nz_r.at[way, step])
                if step < SPLIT - 2:
                    step_on(source, step + 1, way)
                send(slot, slot, np_s.at[source], np_r.at[source], (sp, other), keep=False)

    halves(1)
    pass_on(3)
    hop(0)
    halves(2)
    hop(1)
    halves(3)
    hop(2)
    for dz in range(SPLIT):
        for e in (1, 2):
            source = from_part(dz) * ranks + flip(3)
            landed(gu_at(source, (e - 1) * depth // 2, depth // 2), gh_s.at[dz, e], gh_r.at[dz, e])
            landed(dn_at(source, (e - 1) * width // 2, width // 2), dh_s.at[dz, e], dh_r.at[dz, e])
    locals_[2].wait()
    locals_[3].wait()

    main = width // 128 * 128
    half_lane = width - main

    def feed(source):
        landed(nb.at[source, other], np_s.at[source], np_r.at[source])
        x = nb[source].reshape(rows, nb.shape[-1])
        pieces = []
        gate = jnp.dot(x, wgu[:, pl.ds(0, main)], preferred_element_type=jnp.float32)
        up = jnp.dot(x, wgu[:, pl.ds(main, main)], preferred_element_type=jnp.float32)
        pieces.append((gate / (1.0 + jnp.exp(-gate)) * up).astype(jnp.bfloat16))
        last = jnp.dot(x, wgu[:, pl.ds(2 * main, 128)], preferred_element_type=jnp.float32)
        turned = pltpu.roll(last, half_lane, 1)
        lane = lax.broadcasted_iota(jnp.int32, last.shape, 1)
        tail = jnp.where(lane < half_lane, last / (1.0 + jnp.exp(-last)) * turned, 0.0)
        pieces.append(tail.astype(jnp.bfloat16))
        hidden = jnp.concatenate(pieces, axis=1)
        for first in range(0, wdn.shape[1], tile):
            block = jnp.dot(hidden, wdn[:, first : first + tile], preferred_element_type=jnp.float32)
            dsb[source, :, :, first : first + tile] = block.astype(jnp.bfloat16).reshape(2, share, tile)

    high, odd = part // 2, part % 2
    order = (3 - 3 * high, 2 - 2 * odd + high, 1 + odd, part)
    at_end = (part == 0) | (part == SPLIT - 1)
    inner = (part > 0) & (part < SPLIT - 1)

    def pair_sum(place):
        landed(drv.at[place], dp_s.at[place], dp_r.at[place])
        return dsb[order[place], core].astype(jnp.float32) + drv[place].astype(jnp.float32)

    def onward(place, first):
        target = order[place]
        way = 1 - (target > part).astype(jnp.int32)
        total = pair_sum(place)
        if not first:
            landed(dzb.at[way, target], fz_s.at[way, target], fz_r.at[way, target])
            total = total + dzb[way, target].astype(jnp.float32)
        ds2[target] = total.astype(jnp.bfloat16)
        slot = dzb.at[way, target]
        sender = fz_s.at[way, target]
        send(ds2.at[target], slot, sender, fz_r.at[way, target], (sp + ranks * (1 - 2 * way), core), keep=False)

    for place in range(SPLIT):
        feed(order[place])
        send(dsb.at[order[place], other], drv.at[place], dp_s.at[place], dp_r.at[place], (sp, other))
        if place:

            @pl.when(at_end)
            def _():
                onward(place - 1, True)

    @pl.when(inner)
    def _():
        for place in range(SPLIT - 1):
            onward(place, False)

    acc[...] = pair_sum(SPLIT - 1)
    for way, some in ((0, part > 0), (1, part < SPLIT - 1)):

        @pl.when(some)
        def _():
            landed(dzb.at[way, part], fz_s.at[way, part], fz_r.at[way, part])
            acc[...] += dzb[way, part].astype(jnp.float32)

    down = acc[...]
    out_ref[...] = (st[...].astype(jnp.float32) + 0.5 * down).astype(jnp.bfloat16)
    for copy in sent:
        copy.wait_send()

    def left(src, s_sem, r_sem):
        pltpu.make_async_remote_copy(
            src_ref=src, dst_ref=src, send_sem=s_sem, recv_sem=r_sem, device_id=(sp, other), device_id_type=MESH
        ).wait_send()

    for way in (0, 1):
        for step in range(SPLIT - 1):
            source, there = present(way, step)

            @pl.when(there)
            def _():
                left(nb.at[source, core], np_s.at[source], np_r.at[source])

        for step in range(SPLIT - 1):
            source = part + ahead[way][2] * step

            @pl.when(ahead[way][0] & (source >= 0) & (source < SPLIT))
            def _():
                left(nb.at[source, core], nz_s.at[way, step], nz_r.at[way, step])

    for place in range(SPLIT - 1):
        target = order[place]
        way = 1 - (target > part).astype(jnp.int32)
        left(ds2.at[target], fz_s.at[way, target], fz_r.at[way, target])


def run_layer(key, value, query, k_gain, q_gain, gate, up, down, out_weight, resid, gain, ranks):
    rows = query.shape[0]
    share = rows // 2
    model = resid.shape[1]
    width = down.shape[0] // SPLIT
    depth = gate.shape[0]
    head_dim = q_gain.shape[0]
    n_sp = ranks * SPLIT
    quarter = head_dim // 4
    steps = np.tile(np.arange(quarter, dtype=np.float32), 4)
    freq = jnp.asarray((np.float64(10000.0) ** (-steps / quarter)).astype(np.float32))[None, :]
    half = jnp.bfloat16
    dma = pltpu.SemaphoreType.DMA
    per_part = [dma((SPLIT,))] * 2
    per_near = [dma((SPLIT, 4))] * 2
    per_way = [dma((2, SPLIT))] * 2
    anywhere = pl.BlockSpec(memory_space=pl.ANY)
    inside = pl.BlockSpec(memory_space=pltpu.VMEM)
    kv_shape = (SPLIT, rows, 2 * head_dim)
    q_shape = (SPLIT, rows, query.shape[1] // SPLIT)
    return pl.pallas_call(
        functools.partial(layer_kernel, ranks, head_dim),
        out_shape=jax.ShapeDtypeStruct((share, model), half),
        in_specs=[inside] * 8 + [anywhere] + [inside] * 3,
        out_specs=inside,
        scratch_shapes=[
            pltpu.VMEM((SPLIT, ranks, rows, 2 * head_dim), half),
            pltpu.VMEM(q_shape, half),
            pltpu.VMEM(q_shape, half),
            pltpu.VMEM(q_shape, half),
            pltpu.VMEM((n_sp * depth, 2 * width), half),
            pltpu.VMEM((-(-width // 128) * 128, model), half),
            pltpu.VMEM((2, share, model), half),
            pltpu.VMEM((share, model), half),
            pltpu.VMEM((SPLIT, 2, share, model), half),
            pltpu.VMEM((share, model), half),
            pltpu.VMEM((SPLIT, 2, share, model), half),
            pltpu.VMEM((SPLIT, share, model), half),
            pltpu.VMEM((SPLIT, share, model), half),
            pltpu.VMEM((2, SPLIT, share, model), half),
            pltpu.VMEM((share, model), jnp.float32),
            pltpu.VMEM(kv_shape, half),
            pltpu.VMEM(q_shape, half),
            pltpu.VMEM((SPLIT, depth, 2 * width), half),
            dma((4,)),
        ]
        + per_part + per_near + per_part * 3
        + per_near * 4
        + per_part + [dma, dma] + per_way + per_part * 2 + per_way,
        compiler_params=pltpu.CompilerParams(
            collective_id=0, has_side_effects=True, vmem_limit_bytes=62 * 1024 * 1024
        ),
    )(
        key, value, query, k_gain[None, :], q_gain[None, :], freq, gate, up, down, out_weight, resid, gain[None, :]
    )


def in_kernel(n_sp, n_tp, kv_here, head_dim, width):
    return n_sp == 4 * SPLIT and n_tp == 2 and kv_here == SPLIT and head_dim == 128 and width % 128 == 64


def body(
    resid,
    query,
    key,
    value,
    q_gain,
    k_gain,
    out_weight,
    norm_gain,
    gate_weight,
    up_weight,
    down_weight,
):
    rows = query.shape[0]
    head_dim = q_gain.shape[0]
    heads_here = query.shape[1] // head_dim
    kv_here = key.shape[1] // head_dim
    n_sp = lax.axis_size("sp")
    if not fits(n_sp, kv_here, gate_weight.shape[1]):
        return whole_body(
            resid, query, key, value, q_gain, k_gain, out_weight, norm_gain, gate_weight, up_weight, down_weight
        )
    hidden_part = gate_weight.shape[1] // SPLIT
    ranks = n_sp // SPLIT
    if in_kernel(n_sp, lax.axis_size("tp"), kv_here, head_dim, hidden_part):
        return run_layer(
            key, value, query, k_gain, q_gain, gate_weight, up_weight, down_weight, out_weight, resid, norm_gain, ranks
        )
    tok_groups, hid_groups = groups_of(n_sp)
    ranks = n_sp // SPLIT
    group_size = heads_here // kv_here
    kv_part = kv_here // SPLIT

    def swap(array):
        return lax.all_to_all(array, "sp", 0, 0, axis_index_groups=tok_groups, tiled=True)

    def spread(array, axis):
        return lax.all_gather(array, "sp", axis=axis, axis_index_groups=hid_groups, tiled=True)

    positions = lax.axis_index("sp") * rows + jnp.arange(rows, dtype=jnp.int32)
    q_rot = prepare(query.reshape(rows, heads_here, head_dim), q_gain, positions)
    k_rot = prepare(key.reshape(rows, kv_here, head_dim), k_gain, positions)
    cut = lambda a: a.reshape(a.shape[0], SPLIT, -1).transpose(1, 0, 2).reshape(SPLIT * a.shape[0], -1)
    k_rot, val = cut(k_rot), cut(value)
    pair = swap(jnp.concatenate([k_rot, val], axis=1))
    pair = spread(pair, 0)
    q_mine = swap(cut(q_rot))
    width = kv_part * head_dim
    keys = pair[:, :width].reshape(-1, kv_part, head_dim)
    vals = pair[:, width:].reshape(-1, kv_part, head_dim)
    grouped = q_mine.reshape(SPLIT * rows, kv_part, group_size, head_dim)
    gate_up = spread(swap(jnp.concatenate([cut(gate_weight), cut(up_weight)], axis=1)), 0)
    depth = gate_weight.shape[0]
    gate_up = gate_up.reshape(ranks, SPLIT, depth, -1).transpose(1, 0, 2, 3).reshape(n_sp * depth, -1)
    down_w = swap(down_weight)
    part = down_weight.shape[0] // SPLIT
    down_w = down_w.reshape(SPLIT, part, -1)
    down_w = lax.all_gather(down_w, "sp", axis=1, axis_index_groups=hid_groups)
    down_w = jnp.transpose(down_w, (2, 0, 1, 3)).reshape(part, -1)
    scores = jnp.einsum("qkgd,skd->kgqs", grouped, keys, preferred_element_type=jnp.float32) * head_dim ** (-0.5)
    weights = jnp.exp(scores - jnp.max(scores, axis=-1, keepdims=True))
    totals = jnp.sum(weights, axis=-1)
    accum = jnp.einsum("kgqs,skd->kgqd", weights.astype(jnp.bfloat16), vals, preferred_element_type=jnp.float32)
    attn = jnp.transpose(accum / totals[..., None], (2, 0, 1, 3)).astype(jnp.bfloat16).reshape(SPLIT * rows, -1)
    attn = swap(attn).reshape(SPLIT, rows, -1).transpose(1, 0, 2).reshape(rows, -1)
    return finish(attn, resid, out_weight, norm_gain, gate_up, down_w, tok_groups)


def finish(attn, resid, out_weight, norm_gain, gate_up, down_w, tok_groups):
    rows = resid.shape[0]
    n_tp = lax.axis_size("tp")
    share = rows // n_tp
    my_first = lax.axis_index("tp") * share
    proj = lax.psum_scatter(
        jnp.dot(attn, out_weight, preferred_element_type=jnp.float32).astype(jnp.bfloat16),
        "tp",
        scatter_dimension=0,
        tiled=True,
    ).astype(jnp.float32)
    my_resid = lax.dynamic_slice_in_dim(resid, my_first, share, 0)
    my_stream = (my_resid.astype(jnp.float32) + proj).astype(jnp.bfloat16)
    normed = normalize(my_stream, norm_gain)
    normed = lax.all_gather(normed, "sp", axis=0, axis_index_groups=tok_groups, tiled=False)
    normed = lax.all_gather(normed, "tp", axis=0, tiled=False)
    normed = normed.reshape(n_tp * SPLIT * share, -1)
    both = jnp.dot(normed, gate_up, preferred_element_type=jnp.float32)
    gate, up_part = jnp.split(both, 2, axis=1)
    hidden = (jax.nn.silu(gate) * up_part).astype(jnp.bfloat16)
    down = jnp.dot(hidden, down_w, preferred_element_type=jnp.float32).astype(jnp.bfloat16)
    down = lax.psum_scatter(down, "tp", scatter_dimension=0, tiled=True)
    down = lax.all_to_all(
        down.reshape(SPLIT, share, -1), "sp", 0, 0, axis_index_groups=tok_groups, tiled=True
    )
    down = jnp.sum(down.astype(jnp.float32), axis=0)
    return (my_stream.astype(jnp.float32) + 0.5 * down).astype(jnp.bfloat16)


def solution(mesh):
    placed = (
        P("sp", None),
        P("sp", "tp"),
        P("sp", "tp"),
        P("sp", "tp"),
        P(),
        P(),
        P("tp", None),
        P(),
        P("sp", "tp"),
        P("sp", "tp"),
        P("tp", "sp"),
    )
    return jax.shard_map(
        body, mesh=mesh, in_specs=placed, out_specs=P(("sp", "tp"), None), check_vma=False
    )
```

profile of v0, /device:TPU:0, one launch (start us, length us, event | category | flops | bytes accessed | tf_op | source)
XLA Modules:
  0.0 161.1 jit_solution(8675514288192236901)
XLA Ops:
  0.0 159.3 %shard_map.118 = bf16[96,2048]{1,0:T(8,128)(2,1)} custom-call(bf16[192,512]{1,0:T(8,128)(2,1)} %key_ref.1, bf16[192,512]{1,0:T(8,128)(2,1)} %value_ref.1, bf16[192,1024]{1,0:T(8,128)(2,1)} %query_ref.1, f32[1,128]{1,0:T(1,128)} %bitcast.4, f32[1,128]{1,0:T(1,128)} %bitcast.5, f32[1,128]{1,0:T(1,128)} %constant.3.freq_ref, bf16[128,2816]{1,0:T(8,128)(2,1)} %gate_ref.1, ...), custom_call_target="tpu_custom_call" | custom-call | tf_op jit(solution)/shard_map/pallas_call | solution.py:560
  159.3 1.8 %copy.14 = bf16[96,2048]{1,0:T(8,128)(2,1)} copy(bf16[96,2048]{1,0:T(8,128)(2,1)} %shard_map.118) | data formatting | bytes 786432
where the time goes:
time: 161 us
  Pallas kernels  159 us (99%)
  local copies, waits for them, and re-layouts  1.77 us (1%)
    pallas_call x1, Pallas kernels, run_layer(): pl.pallas_call(functools.partial(layer_kernel, ranks, head_dim), out_shap...  159 us

commit v1 on v0

--- a/solution.py
+++ b/solution.py
@@ -165,10 +165,10 @@
     k_gain_ref,
     q_gain_ref,
     freq_ref,
-    gate_ref,
-    up_ref,
+    gate_hbm,
+    up_hbm,
     down_ref,
-    ow_ref,
+    ow_hbm,
     resid_ref,
     gain_ref,
     out_ref,
@@ -182,18 +182,22 @@
     prv,
     nb,
     st,
+    hb,
     dsb,
     drv,
     ds2,
     dzb,
-    acc,
     kv_ref,
     q_ref,
     gu_ref,
+    gate_ref,
+    up_ref,
+    ow_ref,
     local_sem,
-    kvz_s, kvz_r, kvx_s, kvx_r, q_s, q_r, gz_s, gz_r, dz_s, dz_r,
-    gx_s, gx_r, dx_s, dx_r, gh_s, gh_r, dh_s, dh_r,
-    at_s, at_r, pj_s, pj_r, nz_s, nz_r, np_s, np_r, dp_s, dp_r, fz_s, fz_r,
+    kvp_s, kvp_r, q_s, q_r, qz_s, qz_r, at_r, gz_s, gz_r, dz_s, dz_r, np_s, np_r,
+    gx_s, gx_r, dx_s, dx_r, gh_s, gh_r, dh_s, dh_r, dp_s, dp_r,
+    kvz_s, kvz_r, fz_s, fz_r,
+    nz_s, nz_r, at_s, pj_s, pj_r,
 ):
     sp = lax.axis_index("sp")
     core = lax.axis_index("tp")
@@ -207,6 +211,7 @@
     group = q_ref.shape[2] // head_dim
     other = 1 - core
     flips = (1, 2, 3)
+    last = SPLIT - 1
 
     def flip(e):
         x = rank % 2
@@ -215,24 +220,29 @@
         ny = 1 - y if e // 2 else y
         return ny * 2 + nx
 
-    def peer_part(dz):
-        return ((part + dz) % SPLIT) * ranks + rank
-
-    def from_part(dz):
-        return (part + SPLIT - dz) % SPLIT
-
     def near(e):
         return part * ranks + flip(e)
 
+    def at_part(target):
+        return target * ranks + rank
+
     def dn_own(index):
         return down_ref.at[pl.ds(pl.multiple_of(index * width, 16), width)]
 
     barrier = pltpu.get_barrier_semaphore()
     for dz in range(1, SPLIT):
-        pl.semaphore_signal(barrier, inc=1, device_id=(peer_part(dz), core), device_id_type=MESH)
+        pl.semaphore_signal(barrier, inc=1, device_id=(at_part((part + dz) % SPLIT), core), device_id_type=MESH)
     for e in flips:
         pl.semaphore_signal(barrier, inc=1, device_id=(near(e), core), device_id_type=MESH)
     pl.semaphore_signal(barrier, inc=1, device_id=(sp, other), device_id_type=MESH)
+
+    loads = [
+        pltpu.make_async_copy(gate_hbm, gate_ref, local_sem.at[4]),
+        pltpu.make_async_copy(up_hbm, up_ref, local_sem.at[5]),
+        pltpu.make_async_copy(ow_hbm, ow_ref, local_sem.at[6]),
+    ]
+    for copy in loads:
+        copy.start()
 
     lane = lax.broadcasted_iota(jnp.int32, (rows, head_dim), 1)
     spot = sp * rows + lax.broadcasted_iota(jnp.int32, (rows, head_dim), 0)
@@ -250,13 +260,78 @@
         mate = jnp.where(first_half, pltpu.roll(x, head_dim - quarter, 1), pltpu.roll(x, quarter, 1))
         return (x * cosine + mate * sine).astype(jnp.bfloat16)
 
+    def send(src, dst, s_sem, r_sem, target):
+        copy = pltpu.make_async_remote_copy(
+            src_ref=src, dst_ref=dst, send_sem=s_sem, recv_sem=r_sem, device_id=target, device_id_type=MESH
+        )
+        copy.start()
+
+    def landed(dst, s_sem, r_sem):
+        pltpu.make_async_remote_copy(
+            src_ref=dst, dst_ref=dst, send_sem=s_sem, recv_sem=r_sem, device_id=(sp, other), device_id_type=MESH
+        ).wait_recv()
+
+    def left(src, s_sem, r_sem):
+        pltpu.make_async_remote_copy(
+            src_ref=src, dst_ref=src, send_sem=s_sem, recv_sem=r_sem, device_id=(sp, other), device_id_type=MESH
+        ).wait_send()
+
+    def gu_at(source, first=0, count=None):
+        return wgu.at[pl.ds(pl.multiple_of(source * depth + first, 16), depth if count is None else count)]
+
+    def dn_at(source, first=0, count=None):
+        return wdn.at[pl.ds(first, width if count is None else count), pl.ds(pl.multiple_of(source * cols, cols), cols)]
+
     for index in range(SPLIT):
         kv_ref[index, :, 0:head_dim] = turn(key_ref, index, k_gain_ref)
         kv_ref[index, :, head_dim : 2 * head_dim] = value_ref[:, index * head_dim : (index + 1) * head_dim]
+
+    pl.semaphore_wait(barrier, SPLIT - 1 + 3 + 1)
+
+    ways = ((part < last, 1), (part > 0, -1))
+    kv_ways = (part < last - 1, part > 1)
+    at_end = (part == 0) | (part == last)
+    inner = (part > 0) & (part < last)
+    inward = jnp.where(part == 0, 1, last - 1)
+    outward = jnp.where(part == 1, 0, last)
+
+    def kv_on(way, step, source, piece, src=None):
+        slot = kvb.at[source, piece]
+        send(
+            slot if src is None else src,
+            slot,
+            kvz_s.at[way, step, piece],
+            kvz_r.at[way, step, piece],
+            (sp + ranks * ways[way][1], core),
+        )
+
+    own_kv = kv_ref.at[rank]
+    for e in flips:
+        send(kv_ref.at[flip(e)], kvb.at[part, rank], kvp_s.at[e], kvp_r.at[e], (near(e), core))
+    for way in (0, 1):
+
+        @pl.when(kv_ways[way])
+        def _():
+            kv_on(way, 0, part, rank, own_kv)
+
+    locals_ = [
+        pltpu.make_async_copy(own_kv, kvb.at[part, rank], local_sem.at[0]),
+        pltpu.make_async_copy(dn_own(part), dn_at(sp), local_sem.at[3]),
+    ]
+    for copy in locals_:
+        copy.start()
+
     for index in range(SPLIT):
         for head in range(group):
             lanes = slice(head * head_dim, (head + 1) * head_dim)
             q_ref[index, :, lanes] = turn(query_ref, index * group + head, q_gain_ref)
+    for e in flips:
+        send(q_ref.at[flip(e)], qb.at[0, rank], q_s.at[e], q_r.at[e], (near(e), core))
+    q_own = pltpu.make_async_copy(q_ref.at[rank], qb.at[0, rank], local_sem.at[1])
+    q_own.start()
+
+    loads[0].wait()
+    loads[1].wait()
     whole_lanes = width // 128 * 128
     for index in range(SPLIT):
         start = index * width // 128 * 128
@@ -269,102 +344,118 @@
             gu_ref[index, :, which * whole_lanes : (which + 1) * whole_lanes] = block[:, :whole_lanes]
             rests.append(block[:, whole_lanes:].astype(jnp.float32))
         spread = lax.broadcasted_iota(jnp.int32, rests[0].shape, 1)
-        last = jnp.where(spread < width - whole_lanes, rests[0], pltpu.roll(rests[1], width - whole_lanes, 1))
-        gu_ref[index, :, 2 * whole_lanes :] = last.astype(jnp.bfloat16)
-
-    sent = []
-
-    def send(src, dst, s_sem, r_sem, target, keep=True):
-        copy = pltpu.make_async_remote_copy(
-            src_ref=src, dst_ref=dst, send_sem=s_sem, recv_sem=r_sem, device_id=target, device_id_type=MESH
-        )
-        copy.start()
-        if keep:
-            sent.append(copy)
-        return copy
-
-    def landed(dst, s_sem, r_sem):
-        pltpu.make_async_remote_copy(
-            src_ref=dst, dst_ref=dst, send_sem=s_sem, recv_sem=r_sem, device_id=(sp, other), device_id_type=MESH
-        ).wait_recv()
-
-    def gu_at(source, first=0, count=None):
-        return wgu.at[pl.ds(pl.multiple_of(source * depth + first, 16), depth if count is None else count)]
-
-    def dn_at(source, first=0, count=None):
-        return wdn.at[pl.ds(first, width if count is None else count), pl.ds(pl.multiple_of(source * cols, cols), cols)]
-
-    locals_ = [
-        pltpu.make_async_copy(kv_ref.at[part], kvb.at[part, rank], local_sem.at[0]),
-        pltpu.make_async_copy(q_ref.at[part], qb.at[part], local_sem.at[1]),
-        pltpu.make_async_copy(gu_ref.at[part], gu_at(sp), local_sem.at[2]),
-        pltpu.make_async_copy(dn_own(part), dn_at(sp), local_sem.at[3]),
-    ]
-    for copy in locals_:
-        copy.start()
+        tail = jnp.where(spread < width - whole_lanes, rests[0], pltpu.roll(rests[1], width - whole_lanes, 1))
+        gu_ref[index, :, 2 * whole_lanes :] = tail.astype(jnp.bfloat16)
+    gu_own = pltpu.make_async_copy(gu_ref.at[part], gu_at(sp), local_sem.at[2])
+    gu_own.start()
     pad = wdn.shape[0] - width
     wdn[pl.ds(width, pad), :] = jnp.zeros((pad, wdn.shape[1]), wdn.dtype)
-
-    pl.semaphore_wait(barrier, SPLIT - 1 + 3 + 1)
-
-    def to_part(dz):
-        return (part + dz) % SPLIT
-
-    for dz in range(1, SPLIT):
-        send(kv_ref.at[to_part(dz)], kvb.at[part, rank], kvz_s.at[dz], kvz_r.at[dz], (peer_part(dz), core))
+    for e in (1, 2):
+        send(gu_ref.at[part], gu_at(sp), gx_s.at[part, e], gx_r.at[part, e], (near(e), core))
+    for e in (1, 2):
+        send(dn_own(part), dn_at(sp), dx_s.at[part, e], dx_r.at[part, e], (near(e), core))
+
+    def gate_to(target):
+        @pl.when((target >= 0) & (target < SPLIT))
+        def _():
+            send(gu_ref.at[target], gu_at(sp), gz_s.at[target], gz_r.at[part], (at_part(target), core))
+
+    def down_to(target):
+        @pl.when((target >= 0) & (target < SPLIT))
+        def _():
+            send(dn_own(target), dn_at(sp), dz_s.at[target], dz_r.at[part], (at_part(target), core))
+
+    def downs_in(stage):
+        for way, behind in ((0, part), (1, last - part)):
+
+            @pl.when((behind == stage) & (stage < SPLIT - 2))
+            def _():
+                for d in flips:
+                    down_to(part + d * ways[way][1])
+
+    def gu_pass(source):
+        place = gu_at(at_part(source))
+        landed(place, gz_s.at[source], gz_r.at[source])
+        for e in (1, 2):
+            send(place, place, gx_s.at[source, e], gx_r.at[source, e], (near(e), core))
+
+    def dn_pass(source):
+        place = dn_at(at_part(source))
+        landed(place, dz_s.at[source], dz_r.at[source])
+        for e in (1, 2):
+            send(place, place, dx_s.at[source, e], dx_r.at[source, e], (near(e), core))
+
+    def gu_halves(source):
+        for e in (1, 2):
+            origin = source * ranks + flip(e)
+            landed(gu_at(origin), gx_s.at[source, e], gx_r.at[source, e])
+            half = gu_at(origin, (e - 1) * depth // 2, depth // 2)
+            send(half, half, gh_s.at[source, e], gh_r.at[source, e], (near(3 - e), core))
+
+    def dn_halves(source):
+        for e in (1, 2):
+            origin = source * ranks + flip(e)
+            landed(dn_at(origin), dx_s.at[source, e], dx_r.at[source, e])
+            half = dn_at(origin, (e - 1) * width // 2, width // 2)
+            send(half, half, dh_s.at[source, e], dh_r.at[source, e], (near(3 - e), core))
+
+    def gu_done(source):
+        for e in (1, 2):
+            origin = source * ranks + flip(3)
+            landed(gu_at(origin, (e - 1) * depth // 2, depth // 2), gh_s.at[source, e], gh_r.at[source, e])
+
+    def dn_done(source):
+        for e in (1, 2):
+            origin = source * ranks + flip(3)
+            landed(dn_at(origin, (e - 1) * width // 2, width // 2), dh_s.at[source, e], dh_r.at[source, e])
+
+    high, odd = part // 2, part % 2
+    nears = (part + 1 - 2 * odd, 2 - high, 3 - 3 * high)
+
+    def present(way, step):
+        source = part - ways[way][1] * (step + 1)
+        return source, (source >= 0) & (source < SPLIT)
+
+    def kv_hop(step):
+        for way in (0, 1):
+            source, there = present(way, step)
+
+            @pl.when(there & inner)
+            def _():
+                for piece in range(ranks):
+                    landed(kvb.at[source, piece], kvz_s.at[way, step, piece], kvz_r.at[way, step, piece])
+                    if step == 0:
+
+                        @pl.when(kv_ways[way])
+                        def _():
+                            kv_on(way, 1, source, piece)
+
+    @pl.when(inner)
+    def _():
+        gate_to(outward)
+        down_to(outward)
+
     for e in flips:
-        send(kv_ref.at[part], kvb.at[part, rank], kvx_s.at[0, e], kvx_r.at[0, e], (near(e), core))
-    for dz in range(1, SPLIT):
-        send(q_ref.at[to_part(dz)], qb.at[part], q_s.at[dz], q_r.at[dz], (peer_part(dz), core))
-    for e in (1, 2):
-        send(dn_own(part), dn_at(sp), dx_s.at[0, e], dx_r.at[0, e], (near(e), core))
-    for dz in range(1, SPLIT):
-        send(gu_ref.at[to_part(dz)], gu_at(sp), gz_s.at[dz], gz_r.at[dz], (peer_part(dz), core))
-        send(dn_own(to_part(dz)), dn_at(sp), dz_s.at[dz], dz_r.at[dz], (peer_part(dz), core))
-    for dz in range(1, SPLIT):
-        slot = kvb.at[from_part(dz), rank]
-        landed(slot, kvz_s.at[dz], kvz_r.at[dz])
-        for e in flips:
-            send(slot, slot, kvx_s.at[dz, e], kvx_r.at[dz, e], (near(e), core))
-    for e in (1, 2):
-        send(gu_ref.at[part], gu_at(sp), gx_s.at[0, e], gx_r.at[0, e], (near(e), core))
-
-    def pass_on(dz):
-        source = from_part(dz) * ranks + rank
-        landed(gu_at(source), gz_s.at[dz], gz_r.at[dz])
-        for e in (1, 2):
-            send(gu_at(source), gu_at(source), gx_s.at[dz, e], gx_r.at[dz, e], (near(e), core))
-        landed(dn_at(source), dz_s.at[dz], dz_r.at[dz])
-        for e in (1, 2):
-            send(dn_at(source), dn_at(source), dx_s.at[dz, e], dx_r.at[dz, e], (near(e), core))
-
-    def halves(dz):
-        for e in (1, 2):
-            source = from_part(dz) * ranks + flip(e)
-            across = (near(3 - e), core)
-            landed(gu_at(source), gx_s.at[dz, e], gx_r.at[dz, e])
-            half = gu_at(source, (e - 1) * depth // 2, depth // 2)
-            send(half, half, gh_s.at[dz, e], gh_r.at[dz, e], across)
-            landed(dn_at(source), dx_s.at[dz, e], dx_r.at[dz, e])
-            half = dn_at(source, (e - 1) * width // 2, width // 2)
-            send(half, half, dh_s.at[dz, e], dh_r.at[dz, e], across)
-
-    for dz in range(SPLIT):
-        for e in flips:
-            landed(kvb.at[from_part(dz), flip(e)], kvx_s.at[dz, e], kvx_r.at[dz, e])
+        landed(kvb.at[part, flip(e)], kvp_s.at[e], kvp_r.at[e])
+        for way in (0, 1):
+
+            @pl.when(kv_ways[way])
+            def _():
+                kv_on(way, 0, part, flip(e))
+
     locals_[0].wait()
-    locals_[1].wait()
-    for dz in range(1, SPLIT):
-        landed(qb.at[from_part(dz)], q_s.at[dz], q_r.at[dz])
+    q_own.wait()
+    for e in flips:
+        landed(qb.at[0, flip(e)], q_s.at[e], q_r.at[e])
 
     factor = head_dim ** (-0.5) * math.log2(math.e)
     length = SPLIT * ranks * rows
 
-    def attend(source, target):
+    def attend(plane, piece, target):
         @pl.loop(0, group)
         def _(head):
             lanes = pl.ds(pl.multiple_of(head * head_dim, head_dim), head_dim)
-            q = qb[source, :, lanes]
+            q = qb[plane, piece, :, lanes]
             keys = kvb[:, :, :, pl.ds(0, head_dim)].reshape(length, head_dim)
             scores = lax.dot_general(q, keys, (((1,), (1,)), ((), ())), preferred_element_type=jnp.float32)
             peak = jnp.max(scores, axis=-1, keepdims=True)
@@ -374,15 +465,77 @@
             summed = jnp.dot(weights.astype(jnp.bfloat16), vals, preferred_element_type=jnp.float32)
             target[:, lanes] = (summed / total).astype(jnp.bfloat16)
 
-    for dz in (1, 2, 3):
-        attend(to_part(dz), asend.at[dz])
-        send(asend.at[dz], ab.at[part], at_s.at[dz], at_r.at[dz], (peer_part(dz), core))
-        if dz == 2:
-            pass_on(1)
-    attend(part, ab.at[part])
-    halves(0)
-    for dz in range(1, SPLIT):
-        landed(ab.at[from_part(dz)], at_s.at[dz], at_r.at[dz])
+    def attend_away(piece):
+        attend(1, piece, asend.at[1, piece])
+        send(
+            asend.at[1, piece],
+            ab.at[rank],
+            at_s.at[1, piece],
+            at_r.at[rank],
+            (outward * ranks + piece, core),
+        )
+
+
+    @pl.when(at_end)
+    def _():
+        for piece in range(ranks):
+            slot = qb.at[0, piece]
+            send(slot, qb.at[1, piece], qz_s.at[piece], qz_r.at[piece], (at_part(inward), core))
+        for d in flips:
+            gate_to(part + d * jnp.where(part == 0, 1, -1))
+        gu_halves(part)
+        dn_halves(part)
+        gu_pass(nears[0])
+        gu_halves(nears[0])
+        gu_pass(nears[1])
+        gu_halves(nears[1])
+
+    @pl.when(inner)
+    def _():
+        kv_hop(0)
+        for d in (1, 2):
+            gate_to(part + d * jnp.where(part == 1, 1, -1))
+        gu_halves(part)
+        dn_halves(part)
+        kv_hop(1)
+        for piece in range(ranks):
+            landed(qb.at[1, piece], qz_s.at[piece], qz_r.at[piece])
+
+        @pl.loop(0, 2)
+        def _(piece):
+            attend_away(piece)
+
+        gu_pass(nears[0])
+
+        @pl.loop(2, 4)
+        def _(piece):
+            attend_away(piece)
+
+        gu_halves(nears[0])
+
+        @pl.loop(1, 4)
+        def _(turn_by):
+            piece = (rank + turn_by) % ranks
+            attend(0, piece, asend.at[0, piece])
+            send(
+                asend.at[0, piece],
+                ab.at[rank],
+                at_s.at[0, piece],
+                at_r.at[rank],
+                (part * ranks + piece, core),
+                )
+
+        attend(0, rank, ab.at[rank])
+        gu_pass(nears[1])
+        gu_halves(nears[1])
+
+    loads[2].wait()
+    for e in flips:
+        landed(ab.at[flip(e)], at_s.at[0, flip(e)], at_r.at[flip(e)])
+
+    @pl.when(at_end)
+    def _():
+        landed(ab.at[rank], at_s.at[0, rank], at_r.at[rank])
 
     attn = jnp.concatenate([ab[index] for index in range(SPLIT)], axis=1)
     tile = 512
@@ -390,7 +543,6 @@
         block = jnp.dot(attn, ow_ref[:, first : first + tile], preferred_element_type=jnp.float32)
         pj[:, :, first : first + tile] = block.astype(jnp.bfloat16).reshape(2, share, tile)
     send(pj.at[other], prv, pj_s, pj_r, (sp, other))
-    pass_on(2)
     landed(prv, pj_s, pj_r)
     proj = pj[core].astype(jnp.float32) + prv[...].astype(jnp.float32)
     stream = (resid_ref[pl.ds(pl.multiple_of(core * share, 16), share)].astype(jnp.float32) + proj).astype(jnp.bfloat16)
@@ -398,24 +550,20 @@
     wide = stream.astype(jnp.float32)
     level = lax.rsqrt(jnp.mean(wide * wide, axis=-1, keepdims=True) + EPSILON)
     nb[part, core] = (wide * level * gain_ref[...]).astype(jnp.bfloat16)
-    ahead = [(part < SPLIT - 1, sp + ranks, -1), (part > 0, sp - ranks, 1)]
 
     def step_on(source, step, way):
         slot = nb.at[source, core]
-        go, target, _ = ahead[way]
-
-        @pl.when(go)
+
+        @pl.when(ways[way][0])
         def _():
-            send(slot, slot, nz_s.at[way, step], nz_r.at[way, step], (target, core), keep=False)
-
-    def present(way, step):
-        source = part + ahead[way][2] * (step + 1)
-        return source, (source >= 0) & (source < SPLIT)
+            send(slot, slot, nz_s.at[way, step], nz_r.at[way, step], (sp + ranks * ways[way][1], core))
 
     step_on(part, 0, 0)
     step_on(part, 0, 1)
+    downs_in(0)
     mine = nb.at[part, core]
     send(mine, mine, np_s.at[part], np_r.at[part], (sp, other))
+
     def hop(step):
         for way in (0, 1):
             source, there = present(way, step)
@@ -426,22 +574,18 @@
                 landed(slot, nz_s.at[way, step], nz_r.at[way, step])
                 if step < SPLIT - 2:
                     step_on(source, step + 1, way)
-                send(slot, slot, np_s.at[source], np_r.at[source], (sp, other), keep=False)
-
-    halves(1)
-    pass_on(3)
+                send(slot, slot, np_s.at[source], np_r.at[source], (sp, other))
+
     hop(0)
-    halves(2)
+    downs_in(1)
+    gu_pass(nears[2])
+    dn_pass(nears[0])
     hop(1)
-    halves(3)
-    hop(2)
-    for dz in range(SPLIT):
-        for e in (1, 2):
-            source = from_part(dz) * ranks + flip(3)
-            landed(gu_at(source, (e - 1) * depth // 2, depth // 2), gh_s.at[dz, e], gh_r.at[dz, e])
-            landed(dn_at(source, (e - 1) * width // 2, width // 2), dh_s.at[dz, e], dh_r.at[dz, e])
-    locals_[2].wait()
-    locals_[3].wait()
+    gu_halves(nears[2])
+    gu_own.wait()
+    gu_done(part)
+    for source in nears:
+        gu_done(source)
 
     main = width // 128 * 128
     half_lane = width - main
@@ -449,73 +593,116 @@
     def feed(source):
         landed(nb.at[source, other], np_s.at[source], np_r.at[source])
         x = nb[source].reshape(rows, nb.shape[-1])
-        pieces = []
         gate = jnp.dot(x, wgu[:, pl.ds(0, main)], preferred_element_type=jnp.float32)
         up = jnp.dot(x, wgu[:, pl.ds(main, main)], preferred_element_type=jnp.float32)
-        pieces.append((gate / (1.0 + jnp.exp(-gate)) * up).astype(jnp.bfloat16))
-        last = jnp.dot(x, wgu[:, pl.ds(2 * main, 128)], preferred_element_type=jnp.float32)
-        turned = pltpu.roll(last, half_lane, 1)
-        lane = lax.broadcasted_iota(jnp.int32, last.shape, 1)
-        tail = jnp.where(lane < half_lane, last / (1.0 + jnp.exp(-last)) * turned, 0.0)
-        pieces.append(tail.astype(jnp.bfloat16))
-        hidden = jnp.concatenate(pieces, axis=1)
-        for first in range(0, wdn.shape[1], tile):
-            block = jnp.dot(hidden, wdn[:, first : first + tile], preferred_element_type=jnp.float32)
-            dsb[source, :, :, first : first + tile] = block.astype(jnp.bfloat16).reshape(2, share, tile)
-
-    high, odd = part // 2, part % 2
+        hb[source, :, 0:main] = (gate / (1.0 + jnp.exp(-gate)) * up).astype(jnp.bfloat16)
+        rest = jnp.dot(x, wgu[:, pl.ds(2 * main, 128)], preferred_element_type=jnp.float32)
+        turned = pltpu.roll(rest, half_lane, 1)
+        where = lax.broadcasted_iota(jnp.int32, rest.shape, 1)
+        tail = jnp.where(where < half_lane, rest / (1.0 + jnp.exp(-rest)) * turned, 0.0)
+        hb[source, :, main : main + 128] = tail.astype(jnp.bfloat16)
+
+    feed(part)
+    feed(nears[0])
+    dn_halves(nears[0])
+    dn_pass(nears[1])
+    feed(nears[1])
+    dn_halves(nears[1])
+    dn_pass(nears[2])
+    hop(2)
+    feed(nears[2])
+    locals_[1].wait()
+    dn_done(part)
+    dn_done(nears[0])
+    dn_done(nears[1])
+
     order = (3 - 3 * high, 2 - 2 * odd + high, 1 + odd, part)
-    at_end = (part == 0) | (part == SPLIT - 1)
-    inner = (part > 0) & (part < SPLIT - 1)
-
-    def pair_sum(place):
-        landed(drv.at[place], dp_s.at[place], dp_r.at[place])
-        return dsb[order[place], core].astype(jnp.float32) + drv[place].astype(jnp.float32)
-
-    def onward(place, first):
+    wide_cols = ranks * cols
+
+    def pair_sum(b, place):
+        landed(drv.at[b, place], dp_s.at[b, place], dp_r.at[b, place])
+        return dsb[b, order[place], core].astype(jnp.float32) + drv[b, place].astype(jnp.float32)
+
+    def onward(b, place, first):
         target = order[place]
         way = 1 - (target > part).astype(jnp.int32)
-        total = pair_sum(place)
+        total = pair_sum(b, place)
         if not first:
-            landed(dzb.at[way, target], fz_s.at[way, target], fz_r.at[way, target])
-            total = total + dzb[way, target].astype(jnp.float32)
-        ds2[target] = total.astype(jnp.bfloat16)
-        slot = dzb.at[way, target]
-        sender = fz_s.at[way, target]
-        send(ds2.at[target], slot, sender, fz_r.at[way, target], (sp + ranks * (1 - 2 * way), core), keep=False)
-
-    for place in range(SPLIT):
-        feed(order[place])
-        send(dsb.at[order[place], other], drv.at[place], dp_s.at[place], dp_r.at[place], (sp, other))
-        if place:
-
-            @pl.when(at_end)
-            def _():
-                onward(place - 1, True)
-
-    @pl.when(inner)
-    def _():
-        for place in range(SPLIT - 1):
-            onward(place, False)
-
-    acc[...] = pair_sum(SPLIT - 1)
-    for way, some in ((0, part > 0), (1, part < SPLIT - 1)):
-
-        @pl.when(some)
+            landed(dzb.at[b, way, target], fz_s.at[b, way, target], fz_r.at[b, way, target])
+            total = total + dzb[b, way, target].astype(jnp.float32)
+        ds2[b, target] = total.astype(jnp.bfloat16)
+        send(
+            ds2.at[b, target],
+            dzb.at[b, way, target],
+            fz_s.at[b, way, target],
+            fz_r.at[b, way, target],
+            (sp + ranks * (1 - 2 * way), core),
+        )
+
+    def stage(b):
+        for place in range(SPLIT):
+            target = order[place]
+            block = jnp.dot(hb[target], wdn[:, b * wide_cols : (b + 1) * wide_cols], preferred_element_type=jnp.float32)
+            dsb[b, target] = block.astype(jnp.bfloat16).reshape(2, share, wide_cols)
+            send(dsb.at[b, target, other], drv.at[b, place], dp_s.at[b, place], dp_r.at[b, place], (sp, other))
+
+        @pl.when(at_end)
         def _():
-            landed(dzb.at[way, part], fz_s.at[way, part], fz_r.at[way, part])
-            acc[...] += dzb[way, part].astype(jnp.float32)
-
-    down = acc[...]
-    out_ref[...] = (st[...].astype(jnp.float32) + 0.5 * down).astype(jnp.bfloat16)
-    for copy in sent:
-        copy.wait_send()
-
-    def left(src, s_sem, r_sem):
-        pltpu.make_async_remote_copy(
-            src_ref=src, dst_ref=src, send_sem=s_sem, recv_sem=r_sem, device_id=(sp, other), device_id_type=MESH
-        ).wait_send()
-
+            for place in range(last):
+                onward(b, place, True)
+
+        @pl.when(inner)
+        def _():
+            for place in range(last):
+                onward(b, place, False)
+
+    stage(1)
+    stage(2)
+    dn_halves(nears[2])
+    dn_done(nears[2])
+    stage(0)
+    stage(3)
+
+    for b in (1, 2, 0, 3):
+        lanes = slice(b * wide_cols, (b + 1) * wide_cols)
+        acc = pair_sum(b, last)
+        base = st[:, lanes].astype(jnp.float32)
+
+        def add(way, value, b=b):
+            landed(dzb.at[b, way, part], fz_s.at[b, way, part], fz_r.at[b, way, part])
+            return value + dzb[b, way, part].astype(jnp.float32)
+
+        @pl.when(part == 0)
+        def _():
+            out_ref[:, lanes] = (base + 0.5 * add(1, acc)).astype(jnp.bfloat16)
+
+        @pl.when(part == last)
+        def _():
+            out_ref[:, lanes] = (base + 0.5 * add(0, acc)).astype(jnp.bfloat16)
+
+        @pl.when(inner)
+        def _():
+            out_ref[:, lanes] = (base + 0.5 * add(1, add(0, acc))).astype(jnp.bfloat16)
+
+    for e in flips:
+        left(kv_ref.at[flip(e)], kvp_s.at[e], kvp_r.at[e])
+        left(q_ref.at[flip(e)], q_s.at[e], q_r.at[e])
+    for source in range(SPLIT):
+        for e in (1, 2):
+            place = at_part(source)
+            left(gu_at(place), gx_s.at[source, e], gx_r.at[source, e])
+            left(dn_at(place), dx_s.at[source, e], dx_r.at[source, e])
+            left(gu_at(place, 0, depth // 2), gh_s.at[source, e], gh_r.at[source, e])
+            left(dn_at(place, 0, width // 2), dh_s.at[source, e], dh_r.at[source, e])
+    left(prv, pj_s, pj_r)
+    left(mine, np_s.at[part], np_r.at[part])
+    for b in range(SPLIT):
+        for place in range(SPLIT):
+            left(drv.at[b, place], dp_s.at[b, place], dp_r.at[b, place])
+    for dz in range(1, SPLIT):
+        target = (part + dz) % SPLIT
+        left(gu_ref.at[target], gz_s.at[target], gz_r.at[target])
+        left(dn_own(target), dz_s.at[target], dz_r.at[target])
     for way in (0, 1):
         for step in range(SPLIT - 1):
             source, there = present(way, step)
@@ -525,16 +712,36 @@
                 left(nb.at[source, core], np_s.at[source], np_r.at[source])
 
         for step in range(SPLIT - 1):
-            source = part + ahead[way][2] * step
-
-            @pl.when(ahead[way][0] & (source >= 0) & (source < SPLIT))
+            source, there = present(way, step - 1)
+
+            @pl.when(ways[way][0] & there)
             def _():
                 left(nb.at[source, core], nz_s.at[way, step], nz_r.at[way, step])
 
-    for place in range(SPLIT - 1):
-        target = order[place]
-        way = 1 - (target > part).astype(jnp.int32)
-        left(ds2.at[target], fz_s.at[way, target], fz_r.at[way, target])
+            if step < 2:
+
+                @pl.when(kv_ways[way] & there)
+                def _():
+                    for piece in range(ranks):
+                        left(kvb.at[source, piece], kvz_s.at[way, step, piece], kvz_r.at[way, step, piece])
+
+    @pl.when(at_end)
+    def _():
+        for piece in range(ranks):
+            left(qb.at[0, piece], qz_s.at[piece], qz_r.at[piece])
+
+    @pl.when(inner)
+    def _():
+        for piece in range(ranks):
+            left(asend.at[1, piece], at_s.at[1, piece], at_r.at[rank])
+        for e in flips:
+            left(asend.at[0, flip(e)], at_s.at[0, flip(e)], at_r.at[rank])
+
+    for b in range(SPLIT):
+        for place in range(last):
+            target = order[place]
+            way = 1 - (target > part).astype(jnp.int32)
+            left(ds2.at[b, target], fz_s.at[b, way, target], fz_r.at[b, way, target])
 
 
 def run_layer(key, value, query, k_gain, q_gain, gate, up, down, out_weight, resid, gain, ranks):
@@ -550,9 +757,8 @@
     freq = jnp.asarray((np.float64(10000.0) ** (-steps / quarter)).astype(np.float32))[None, :]
     half = jnp.bfloat16
     dma = pltpu.SemaphoreType.DMA
-    per_part = [dma((SPLIT,))] * 2
-    per_near = [dma((SPLIT, 4))] * 2
-    per_way = [dma((2, SPLIT))] * 2
+    padded = -(-width // 128) * 128
+    some = model // SPLIT
     anywhere = pl.BlockSpec(memory_space=pl.ANY)
     inside = pl.BlockSpec(memory_space=pltpu.VMEM)
     kv_shape = (SPLIT, rows, 2 * head_dim)
@@ -560,32 +766,38 @@
     return pl.pallas_call(
         functools.partial(layer_kernel, ranks, head_dim),
         out_shape=jax.ShapeDtypeStruct((share, model), half),
-        in_specs=[inside] * 8 + [anywhere] + [inside] * 3,
+        in_specs=[inside] * 6 + [anywhere] * 4 + [inside] * 2,
         out_specs=inside,
         scratch_shapes=[
             pltpu.VMEM((SPLIT, ranks, rows, 2 * head_dim), half),
-            pltpu.VMEM(q_shape, half),
-            pltpu.VMEM(q_shape, half),
+            pltpu.VMEM((2, *q_shape), half),
+            pltpu.VMEM((2, *q_shape), half),
             pltpu.VMEM(q_shape, half),
             pltpu.VMEM((n_sp * depth, 2 * width), half),
-            pltpu.VMEM((-(-width // 128) * 128, model), half),
+            pltpu.VMEM((padded, model), half),
             pltpu.VMEM((2, share, model), half),
             pltpu.VMEM((share, model), half),
             pltpu.VMEM((SPLIT, 2, share, model), half),
             pltpu.VMEM((share, model), half),
-            pltpu.VMEM((SPLIT, 2, share, model), half),
-            pltpu.VMEM((SPLIT, share, model), half),
-            pltpu.VMEM((SPLIT, share, model), half),
-            pltpu.VMEM((2, SPLIT, share, model), half),
-            pltpu.VMEM((share, model), jnp.float32),
+            pltpu.VMEM((SPLIT, rows, padded), half),
+            pltpu.VMEM((SPLIT, SPLIT, 2, share, some), half),
+            pltpu.VMEM((SPLIT, SPLIT, share, some), half),
+            pltpu.VMEM((SPLIT, SPLIT, share, some), half),
+            pltpu.VMEM((SPLIT, 2, SPLIT, share, some), half),
             pltpu.VMEM(kv_shape, half),
             pltpu.VMEM(q_shape, half),
             pltpu.VMEM((SPLIT, depth, 2 * width), half),
-            dma((4,)),
+            pltpu.VMEM(gate.shape, half),
+            pltpu.VMEM(up.shape, half),
+            pltpu.VMEM(out_weight.shape, half),
+            dma((7,)),
         ]
-        + per_part + per_near + per_part * 3
-        + per_near * 4
-        + per_part + [dma, dma] + per_way + per_part * 2 + per_way,
+        + [dma((SPLIT,))] * 13
+        + [dma((SPLIT, SPLIT))] * 10
+        + [dma((2, SPLIT, ranks))] * 2
+        + [dma((SPLIT, 2, SPLIT))] * 2
+        + [dma((2, SPLIT))] * 3
+        + [dma, dma],
         compiler_params=pltpu.CompilerParams(
             collective_id=0, has_side_effects=True, vmem_limit_bytes=62 * 1024 * 1024
         ),

time: 161 us -> 155 us (0.963)
  Pallas kernels: 159 us -> 153 us
    pallas_call x1, Pallas kernels: 159 us -> 153 us  [run_layer(): pl.pallas_call(functools.partial(layer_kernel, ranks, head_dim), out_shap...]
where the time goes in v1:
time: 155 us; the launch traced here: 154 us
  Pallas kernels  153 us (99%)
  local copies, waits for them, and re-layouts  1.77 us (1%)
    pallas_call x1, Pallas kernels, run_layer(): pl.pallas_call(functools.partial(layer_kernel, ranks, head_dim), out_shap...  153 us

profile of v1, /device:TPU:0, one launch (start us, length us, event | category | flops | bytes accessed | tf_op | source)
XLA Modules:
  0.0 154.4 jit_solution(2776109503154099436)
XLA Ops:
  0.0 152.7 %shard_map.118 = bf16[96,2048]{1,0:T(8,128)(2,1)} custom-call(bf16[192,512]{1,0:T(8,128)(2,1)} %key_ref.1, bf16[192,512]{1,0:T(8,128)(2,1)} %value_ref.1, bf16[192,1024]{1,0:T(8,128)(2,1)} %query_ref.1, f32[1,128]{1,0:T(1,128)} %bitcast.4, f32[1,128]{1,0:T(1,128)} %bitcast.5, f32[1,128]{1,0:T(1,128)} %constant.3.freq_ref, bf16[128,2816]{1,0:T(8,128)(2,1)} %gate_hbm.1, ...), custom_call_target="tpu_custom_call" | custom-call | tf_op jit(solution)/shard_map/pallas_call | solution.py:766
  152.7 1.8 %copy.14 = bf16[96,2048]{1,0:T(8,128)(2,1)} copy(bf16[96,2048]{1,0:T(8,128)(2,1)} %shard_map.118) | data formatting | bytes 786432

commit v2 on v1

--- a/solution.py
+++ b/solution.py
@@ -171,6 +171,7 @@
     ow_hbm,
     resid_ref,
     gain_ref,
+    out_hbm,
     out_ref,
     kvb,
     qb,
@@ -194,10 +195,9 @@
     up_ref,
     ow_ref,
     local_sem,
-    kvp_s, kvp_r, q_s, q_r, qz_s, qz_r, at_r, gz_s, gz_r, dz_s, dz_r, np_s, np_r,
-    gx_s, gx_r, dx_s, dx_r, gh_s, gh_r, dh_s, dh_r, dp_s, dp_r,
-    kvz_s, kvz_r, fz_s, fz_r,
-    nz_s, nz_r, at_s, pj_s, pj_r,
+    kvp_s, q_s, qz_s, gz_s, dz_s, np_s, gx_s, dx_s, gh_s, dh_s, dp_s, fz_s, pj_s, pj_r, gh_r,
+    kvp_r, q_r, qz_r, at_r, gz_r, dz_r, np_r, dh_r,
+    gx_r, dx_r, dp_r, at_s, kvz_s, kvz_r, nz_s, nz_r, fz_r,
 ):
     sp = lax.axis_index("sp")
     core = lax.axis_index("tp")
@@ -307,7 +307,7 @@
 
     own_kv = kv_ref.at[rank]
     for e in flips:
-        send(kv_ref.at[flip(e)], kvb.at[part, rank], kvp_s.at[e], kvp_r.at[e], (near(e), core))
+        send(kv_ref.at[flip(e)], kvb.at[part, rank], kvp_s, kvp_r.at[e], (near(e), core))
     for way in (0, 1):
 
         @pl.when(kv_ways[way])
@@ -326,7 +326,7 @@
             lanes = slice(head * head_dim, (head + 1) * head_dim)
             q_ref[index, :, lanes] = turn(query_ref, index * group + head, q_gain_ref)
     for e in flips:
-        send(q_ref.at[flip(e)], qb.at[0, rank], q_s.at[e], q_r.at[e], (near(e), core))
+        send(q_ref.at[flip(e)], qb.at[0, rank], q_s, q_r.at[e], (near(e), core))
     q_own = pltpu.make_async_copy(q_ref.at[rank], qb.at[0, rank], local_sem.at[1])
     q_own.start()
 
@@ -351,66 +351,52 @@
     pad = wdn.shape[0] - width
     wdn[pl.ds(width, pad), :] = jnp.zeros((pad, wdn.shape[1]), wdn.dtype)
     for e in (1, 2):
-        send(gu_ref.at[part], gu_at(sp), gx_s.at[part, e], gx_r.at[part, e], (near(e), core))
+        send(gu_ref.at[part], gu_at(sp), gx_s, gx_r.at[part, e - 1], (near(e), core))
     for e in (1, 2):
-        send(dn_own(part), dn_at(sp), dx_s.at[part, e], dx_r.at[part, e], (near(e), core))
+        send(dn_own(part), dn_at(sp), dx_s, dx_r.at[part, e - 1], (near(e), core))
 
     def gate_to(target):
         @pl.when((target >= 0) & (target < SPLIT))
         def _():
-            send(gu_ref.at[target], gu_at(sp), gz_s.at[target], gz_r.at[part], (at_part(target), core))
+            send(gu_ref.at[target], gu_at(sp), gz_s, gz_r.at[part], (at_part(target), core))
 
     def down_to(target):
         @pl.when((target >= 0) & (target < SPLIT))
         def _():
-            send(dn_own(target), dn_at(sp), dz_s.at[target], dz_r.at[part], (at_part(target), core))
-
-    def downs_in(stage):
-        for way, behind in ((0, part), (1, last - part)):
-
-            @pl.when((behind == stage) & (stage < SPLIT - 2))
-            def _():
-                for d in flips:
-                    down_to(part + d * ways[way][1])
+            send(dn_own(target), dn_at(sp), dz_s, dz_r.at[part], (at_part(target), core))
 
     def gu_pass(source):
         place = gu_at(at_part(source))
-        landed(place, gz_s.at[source], gz_r.at[source])
+        landed(place, gz_s, gz_r.at[source])
         for e in (1, 2):
-            send(place, place, gx_s.at[source, e], gx_r.at[source, e], (near(e), core))
+            send(place, place, gx_s, gx_r.at[source, e - 1], (near(e), core))
 
     def dn_pass(source):
         place = dn_at(at_part(source))
-        landed(place, dz_s.at[source], dz_r.at[source])
+        landed(place, dz_s, dz_r.at[source])
         for e in (1, 2):
-            send(place, place, dx_s.at[source, e], dx_r.at[source, e], (near(e), core))
+            send(place, place, dx_s, dx_r.at[source, e - 1], (near(e), core))
 
     def gu_halves(source):
         for e in (1, 2):
             origin = source * ranks + flip(e)
-            landed(gu_at(origin), gx_s.at[source, e], gx_r.at[source, e])
+            landed(gu_at(origin), gx_s, gx_r.at[source, e - 1])
             half = gu_at(origin, (e - 1) * depth // 2, depth // 2)
-            send(half, half, gh_s.at[source, e], gh_r.at[source, e], (near(3 - e), core))
+            send(half, half, gh_s, gh_r, (near(3 - e), core))
 
     def dn_halves(source):
         for e in (1, 2):
             origin = source * ranks + flip(e)
-            landed(dn_at(origin), dx_s.at[source, e], dx_r.at[source, e])
+            landed(dn_at(origin), dx_s, dx_r.at[source, e - 1])
             half = dn_at(origin, (e - 1) * width // 2, width // 2)
-            send(half, half, dh_s.at[source, e], dh_r.at[source, e], (near(3 - e), core))
-
-    def gu_done(source):
-        for e in (1, 2):
-            origin = source * ranks + flip(3)
-            landed(gu_at(origin, (e - 1) * depth // 2, depth // 2), gh_s.at[source, e], gh_r.at[source, e])
+            send(half, half, dh_s, dh_r.at[source], (near(3 - e), core))
 
     def dn_done(source):
-        for e in (1, 2):
-            origin = source * ranks + flip(3)
-            landed(dn_at(origin, (e - 1) * width // 2, width // 2), dh_s.at[source, e], dh_r.at[source, e])
+        landed(dn_at(source * ranks + flip(3)), dh_s, dh_r.at[source])
 
     high, odd = part // 2, part % 2
     nears = (part + 1 - 2 * odd, 2 - high, 3 - 3 * high)
+    second, third = jnp.where(inner, nears[2], nears[1]), jnp.where(inner, nears[1], nears[2])
 
     def present(way, step):
         source = part - ways[way][1] * (step + 1)
@@ -436,7 +422,7 @@
         down_to(outward)
 
     for e in flips:
-        landed(kvb.at[part, flip(e)], kvp_s.at[e], kvp_r.at[e])
+        landed(kvb.at[part, flip(e)], kvp_s, kvp_r.at[e])
         for way in (0, 1):
 
             @pl.when(kv_ways[way])
@@ -446,7 +432,7 @@
     locals_[0].wait()
     q_own.wait()
     for e in flips:
-        landed(qb.at[0, flip(e)], q_s.at[e], q_r.at[e])
+        landed(qb.at[0, flip(e)], q_s, q_r.at[e])
 
     factor = head_dim ** (-0.5) * math.log2(math.e)
     length = SPLIT * ranks * rows
@@ -480,41 +466,30 @@
     def _():
         for piece in range(ranks):
             slot = qb.at[0, piece]
-            send(slot, qb.at[1, piece], qz_s.at[piece], qz_r.at[piece], (at_part(inward), core))
-        for d in flips:
-            gate_to(part + d * jnp.where(part == 0, 1, -1))
+            send(slot, qb.at[1, piece], qz_s, qz_r.at[piece], (at_part(inward), core))
+        for target in nears:
+            gate_to(target)
+        down_to(nears[0])
+        gu_pass(nears[0])
         gu_halves(part)
         dn_halves(part)
-        gu_pass(nears[0])
         gu_halves(nears[0])
-        gu_pass(nears[1])
-        gu_halves(nears[1])
+        dn_pass(nears[0])
+        gu_pass(second)
 
     @pl.when(inner)
     def _():
         kv_hop(0)
-        for d in (1, 2):
-            gate_to(part + d * jnp.where(part == 1, 1, -1))
+        gate_to(nears[2])
+        gate_to(nears[1])
+        down_to(nears[2])
+        down_to(nears[1])
         gu_halves(part)
         dn_halves(part)
         kv_hop(1)
         for piece in range(ranks):
-            landed(qb.at[1, piece], qz_s.at[piece], qz_r.at[piece])
-
-        @pl.loop(0, 2)
-        def _(piece):
-            attend_away(piece)
-
-        gu_pass(nears[0])
-
-        @pl.loop(2, 4)
-        def _(piece):
-            attend_away(piece)
-
-        gu_halves(nears[0])
-
-        @pl.loop(1, 4)
-        def _(turn_by):
+            landed(qb.at[1, piece], qz_s, qz_r.at[piece])
+        def attend_near(turn_by):
             piece = (rank + turn_by) % ranks
             attend(0, piece, asend.at[0, piece])
             send(
@@ -523,11 +498,23 @@
                 at_s.at[0, piece],
                 at_r.at[rank],
                 (part * ranks + piece, core),
-                )
-
+            )
+
+
+        @pl.loop(1, 4)
+        def _(turn_by):
+            attend_near(turn_by)
+
+        gu_pass(nears[0])
+
+        @pl.loop(0, 3)
+        def _(piece):
+            attend_away(piece)
+
+        gu_pass(second)
+        attend_away(3)
         attend(0, rank, ab.at[rank])
-        gu_pass(nears[1])
-        gu_halves(nears[1])
+        gu_halves(nears[0])
 
     loads[2].wait()
     for e in flips:
@@ -560,38 +547,29 @@
 
     step_on(part, 0, 0)
     step_on(part, 0, 1)
-    downs_in(0)
     mine = nb.at[part, core]
-    send(mine, mine, np_s.at[part], np_r.at[part], (sp, other))
-
-    def hop(step):
+    send(mine, mine, np_s, np_r.at[part], (sp, other))
+
+    def hop(step, chosen=(True, True)):
         for way in (0, 1):
             source, there = present(way, step)
 
-            @pl.when(there)
+            @pl.when(there & chosen[way])
             def _():
                 slot = nb.at[source, core]
                 landed(slot, nz_s.at[way, step], nz_r.at[way, step])
                 if step < SPLIT - 2:
                     step_on(source, step + 1, way)
-                send(slot, slot, np_s.at[source], np_r.at[source], (sp, other))
-
-    hop(0)
-    downs_in(1)
-    gu_pass(nears[2])
-    dn_pass(nears[0])
-    hop(1)
-    gu_halves(nears[2])
-    gu_own.wait()
-    gu_done(part)
-    for source in nears:
-        gu_done(source)
+                send(slot, slot, np_s, np_r.at[source], (sp, other))
+
+    outer = (at_end | (high == 0), at_end | (high == 1))
+    across = (inner & (high == 1), inner & (high == 0))
 
     main = width // 128 * 128
     half_lane = width - main
 
     def feed(source):
-        landed(nb.at[source, other], np_s.at[source], np_r.at[source])
+        landed(nb.at[source, other], np_s, np_r.at[source])
         x = nb[source].reshape(rows, nb.shape[-1])
         gate = jnp.dot(x, wgu[:, pl.ds(0, main)], preferred_element_type=jnp.float32)
         up = jnp.dot(x, wgu[:, pl.ds(main, main)], preferred_element_type=jnp.float32)
@@ -602,74 +580,109 @@
         tail = jnp.where(where < half_lane, rest / (1.0 + jnp.exp(-rest)) * turned, 0.0)
         hb[source, :, main : main + 128] = tail.astype(jnp.bfloat16)
 
-    feed(part)
-    feed(nears[0])
+    order = nears + (part,)
+    wide_cols = ranks * cols
+    first_cols, later_cols = (1, 2), (0, 3)
+
+    def pair_sum(b, place):
+        landed(drv.at[b, place], dp_s, dp_r.at[b, place])
+        return dsb[b, order[place], core].astype(jnp.float32) + drv[b, place].astype(jnp.float32)
+
+    def onward(blocks, place, first):
+        target = order[place]
+        way = 1 - (target > part).astype(jnp.int32)
+        for b in blocks:
+            total = pair_sum(b, place)
+            if not first:
+                landed(dzb.at[b, way, target], fz_s, fz_r.at[b, way, target])
+                total = total + dzb[b, way, target].astype(jnp.float32)
+            ds2[b, target] = total.astype(jnp.bfloat16)
+            send(
+                ds2.at[b, target],
+                dzb.at[b, way, target],
+                fz_s,
+                fz_r.at[b, way, target],
+                (sp + ranks * (1 - 2 * way), core),
+            )
+
+    def stage(blocks, place):
+        target = order[place]
+        for b in blocks:
+            block = jnp.dot(hb[target], wdn[:, b * wide_cols : (b + 1) * wide_cols], preferred_element_type=jnp.float32)
+            dsb[b, target] = block.astype(jnp.bfloat16).reshape(2, share, wide_cols)
+            send(dsb.at[b, target, other], drv.at[b, place], dp_s, dp_r.at[b, place], (sp, other))
+
+    def ends_on(blocks, place):
+        @pl.when(at_end)
+        def _():
+            onward(blocks, place, True)
+
+    gu_halves(second)
+    gu_pass(third)
+
+    @pl.when(inner)
+    def _():
+        dn_pass(nears[0])
+
+    hop(0, outer)
+
+    @pl.when(at_end)
+    def _():
+        down_to(nears[1])
+        down_to(nears[2])
+
+    gu_halves(third)
     dn_halves(nears[0])
     dn_pass(nears[1])
-    feed(nears[1])
+    gu_own.wait()
+    landed(gu_at(0, 0, ranks * depth), gh_s, gh_r)
+    feed(nears[0])
+    hop(0, across)
+    feed(part)
     dn_halves(nears[1])
-    dn_pass(nears[2])
-    hop(2)
-    feed(nears[2])
     locals_[1].wait()
     dn_done(part)
     dn_done(nears[0])
     dn_done(nears[1])
-
-    order = (3 - 3 * high, 2 - 2 * odd + high, 1 + odd, part)
-    wide_cols = ranks * cols
-
-    def pair_sum(b, place):
-        landed(drv.at[b, place], dp_s.at[b, place], dp_r.at[b, place])
-        return dsb[b, order[place], core].astype(jnp.float32) + drv[b, place].astype(jnp.float32)
-
-    def onward(b, place, first):
-        target = order[place]
-        way = 1 - (target > part).astype(jnp.int32)
-        total = pair_sum(b, place)
-        if not first:
-            landed(dzb.at[b, way, target], fz_s.at[b, way, target], fz_r.at[b, way, target])
-            total = total + dzb[b, way, target].astype(jnp.float32)
-        ds2[b, target] = total.astype(jnp.bfloat16)
-        send(
-            ds2.at[b, target],
-            dzb.at[b, way, target],
-            fz_s.at[b, way, target],
-            fz_r.at[b, way, target],
-            (sp + ranks * (1 - 2 * way), core),
-        )
-
-    def stage(b):
-        for place in range(SPLIT):
-            target = order[place]
-            block = jnp.dot(hb[target], wdn[:, b * wide_cols : (b + 1) * wide_cols], preferred_element_type=jnp.float32)
-            dsb[b, target] = block.astype(jnp.bfloat16).reshape(2, share, wide_cols)
-            send(dsb.at[b, target, other], drv.at[b, place], dp_s.at[b, place], dp_r.at[b, place], (sp, other))
-
-        @pl.when(at_end)
-        def _():
-            for place in range(last):
-                onward(b, place, True)
-
-        @pl.when(inner)
-        def _():
-            for place in range(last):
-                onward(b, place, False)
-
-    stage(1)
-    stage(2)
+    stage(first_cols, 0)
+    stage(first_cols, 3)
+    ends_on(first_cols, 0)
+    hop(1)
+    feed(nears[1])
+    stage(first_cols, 1)
+    dn_pass(nears[2])
+    ends_on(first_cols, 1)
+    hop(2)
+    feed(nears[2])
+    stage(first_cols, 2)
     dn_halves(nears[2])
+    ends_on(first_cols, 2)
+
+    @pl.when(inner)
+    def _():
+        onward(first_cols, 1, False)
+
     dn_done(nears[2])
-    stage(0)
-    stage(3)
-
-    for b in (1, 2, 0, 3):
+    stage(later_cols, 0)
+    stage(later_cols, 1)
+    ends_on(later_cols, 0)
+    stage(later_cols, 2)
+    ends_on(later_cols, 1)
+    stage(later_cols, 3)
+    ends_on(later_cols, 2)
+
+    @pl.when(inner)
+    def _():
+        for blocks, place in ((first_cols, 2), (first_cols, 0), (later_cols, 1), (later_cols, 2), (later_cols, 0)):
+            onward(blocks, place, False)
+
+    for b in first_cols + later_cols:
         lanes = slice(b * wide_cols, (b + 1) * wide_cols)
         acc = pair_sum(b, last)
         base = st[:, lanes].astype(jnp.float32)
 
         def add(way, value, b=b):
-            landed(dzb.at[b, way, part], fz_s.at[b, way, part], fz_r.at[b, way, part])
+            landed(dzb.at[b, way, part], fz_s, fz_r.at[b, way, part])
             return value + dzb[b, way, part].astype(jnp.float32)
 
         @pl.when(part == 0)
@@ -684,33 +697,21 @@
         def _():
             out_ref[:, lanes] = (base + 0.5 * add(1, add(0, acc))).astype(jnp.bfloat16)
 
-    for e in flips:
-        left(kv_ref.at[flip(e)], kvp_s.at[e], kvp_r.at[e])
-        left(q_ref.at[flip(e)], q_s.at[e], q_r.at[e])
-    for source in range(SPLIT):
-        for e in (1, 2):
-            place = at_part(source)
-            left(gu_at(place), gx_s.at[source, e], gx_r.at[source, e])
-            left(dn_at(place), dx_s.at[source, e], dx_r.at[source, e])
-            left(gu_at(place, 0, depth // 2), gh_s.at[source, e], gh_r.at[source, e])
-            left(dn_at(place, 0, width // 2), dh_s.at[source, e], dh_r.at[source, e])
+        pltpu.make_async_copy(out_ref.at[:, lanes], out_hbm.at[:, lanes], local_sem.at[7 + b]).start()
+
+    left(kv_ref.at[pl.ds(0, last)], kvp_s, kvp_r.at[1])
+    left(q_ref.at[pl.ds(0, last)], q_s, q_r.at[1])
+    left(gu_ref.at[pl.ds(0, last)], gz_s, gz_r.at[0])
+    left(down_ref.at[pl.ds(0, last * width)], dz_s, dz_r.at[0])
+    left(gu_at(0, 0, 2 * ranks * depth), gx_s, gx_r.at[0, 0])
+    left(gu_at(0, 0, ranks * depth), gh_s, gh_r)
+    left(wdn.at[pl.ds(0, width), pl.ds(0, 2 * wide_cols)], dx_s, dx_r.at[0, 0])
+    left(wdn.at[pl.ds(0, width), pl.ds(0, wide_cols)], dh_s, dh_r.at[0])
     left(prv, pj_s, pj_r)
-    left(mine, np_s.at[part], np_r.at[part])
-    for b in range(SPLIT):
-        for place in range(SPLIT):
-            left(drv.at[b, place], dp_s.at[b, place], dp_r.at[b, place])
-    for dz in range(1, SPLIT):
-        target = (part + dz) % SPLIT
-        left(gu_ref.at[target], gz_s.at[target], gz_r.at[target])
-        left(dn_own(target), dz_s.at[target], dz_r.at[target])
+    left(nb.at[:, 0], np_s, np_r.at[0])
+    left(drv, dp_s, dp_r.at[0, 0])
+    left(drv.at[pl.ds(0, last)], fz_s, fz_r.at[0, 0, 0])
     for way in (0, 1):
-        for step in range(SPLIT - 1):
-            source, there = present(way, step)
-
-            @pl.when(there)
-            def _():
-                left(nb.at[source, core], np_s.at[source], np_r.at[source])
-
         for step in range(SPLIT - 1):
             source, there = present(way, step - 1)
 
@@ -727,8 +728,7 @@
 
     @pl.when(at_end)
     def _():
-        for piece in range(ranks):
-            left(qb.at[0, piece], qz_s.at[piece], qz_r.at[piece])
+        left(qb.at[0], qz_s, qz_r.at[0])
 
     @pl.when(inner)
     def _():
@@ -738,10 +738,8 @@
             left(asend.at[0, flip(e)], at_s.at[0, flip(e)], at_r.at[rank])
 
     for b in range(SPLIT):
-        for place in range(last):
-            target = order[place]
-            way = 1 - (target > part).astype(jnp.int32)
-            left(ds2.at[b, target], fz_s.at[b, way, target], fz_r.at[b, way, target])
+        lanes = slice(b * wide_cols, (b + 1) * wide_cols)
+        pltpu.make_async_copy(out_ref.at[:, lanes], out_hbm.at[:, lanes], local_sem.at[7 + b]).wait()
 
 
 def run_layer(key, value, query, k_gain, q_gain, gate, up, down, out_weight, resid, gain, ranks):
@@ -767,8 +765,9 @@
         functools.partial(layer_kernel, ranks, head_dim),
         out_shape=jax.ShapeDtypeStruct((share, model), half),
         in_specs=[inside] * 6 + [anywhere] * 4 + [inside] * 2,
-        out_specs=inside,
+        out_specs=anywhere,
         scratch_shapes=[
+            pltpu.VMEM((share, model), half),
             pltpu.VMEM((SPLIT, ranks, rows, 2 * head_dim), half),
             pltpu.VMEM((2, *q_shape), half),
             pltpu.VMEM((2, *q_shape), half),
@@ -790,14 +789,15 @@
             pltpu.VMEM(gate.shape, half),
             pltpu.VMEM(up.shape, half),
             pltpu.VMEM(out_weight.shape, half),
-            dma((7,)),
+            dma((7 + SPLIT,)),
         ]
-        + [dma((SPLIT,))] * 13
-        + [dma((SPLIT, SPLIT))] * 10
-        + [dma((2, SPLIT, ranks))] * 2
-        + [dma((SPLIT, 2, SPLIT))] * 2
-        + [dma((2, SPLIT))] * 3
-        + [dma, dma],
+        + [dma] * 15
+        + [dma((SPLIT,))] * 8
+        + [dma((SPLIT, 2))] * 2
+        + [dma((SPLIT, SPLIT)), dma((2, SPLIT))]
+        + [dma((2, 2, ranks))] * 2
+        + [dma((2, SPLIT - 1))] * 2
+        + [dma((SPLIT, 2, SPLIT))],
         compiler_params=pltpu.CompilerParams(
             collective_id=0, has_side_effects=True, vmem_limit_bytes=62 * 1024 * 1024
         ),

time: 155 us -> 136 us (0.88)
  Pallas kernels: 153 us -> 134 us
    pallas_call x1, Pallas kernels: 153 us -> 134 us  [run_layer(): pl.pallas_call(functools.partial(layer_kernel, ranks, head_dim), out_shap...]
where the time goes in v2:
time: 136 us; the launch traced here: 135 us
  Pallas kernels  134 us (99%)
  local copies, waits for them, and re-layouts  1.77 us (1%)
    pallas_call x1, Pallas kernels, run_layer(): pl.pallas_call(functools.partial(layer_kernel, ranks, head_dim), out_shap...  134 us

profile of v2, /device:TPU:0, one launch (start us, length us, event | category | flops | bytes accessed | tf_op | source)
XLA Modules:
  0.0 135.5 jit_solution(9409701767790757603)
XLA Ops:
  0.0 133.7 %shard_map.118 = bf16[96,2048]{1,0:T(8,128)(2,1)} custom-call(bf16[192,512]{1,0:T(8,128)(2,1)} %key_ref.1, bf16[192,512]{1,0:T(8,128)(2,1)} %value_ref.1, bf16[192,1024]{1,0:T(8,128)(2,1)} %query_ref.1, f32[1,128]{1,0:T(1,128)} %bitcast.4, f32[1,128]{1,0:T(1,128)} %bitcast.5, f32[1,128]{1,0:T(1,128)} %constant.3.freq_ref, bf16[128,2816]{1,0:T(8,128)(2,1)} %gate_hbm.1, ...), custom_call_target="tpu_custom_call" | custom-call | tf_op jit(solution)/shard_map/pallas_call | solution.py:764
  133.7 1.8 %copy.14 = bf16[96,2048]{1,0:T(8,128)(2,1)} copy(bf16[96,2048]{1,0:T(8,128)(2,1)} %shard_map.118) | data formatting | bytes 786432

commit v3 on v2

--- a/solution.py
+++ b/solution.py
@@ -352,8 +352,15 @@
     wdn[pl.ds(width, pad), :] = jnp.zeros((pad, wdn.shape[1]), wdn.dtype)
     for e in (1, 2):
         send(gu_ref.at[part], gu_at(sp), gx_s, gx_r.at[part, e - 1], (near(e), core))
-    for e in (1, 2):
-        send(dn_own(part), dn_at(sp), dx_s, dx_r.at[part, e - 1], (near(e), core))
+
+    def own_downs():
+        for e in (1, 2):
+            send(dn_own(part), dn_at(sp), dx_s, dx_r.at[part, e - 1], (near(e), core))
+
+    @pl.when(inner)
+    def _():
+        own_downs()
+
 
     def gate_to(target):
         @pl.when((target >= 0) & (target < SPLIT))
@@ -428,6 +435,11 @@
             @pl.when(kv_ways[way])
             def _():
                 kv_on(way, 0, part, flip(e))
+
+
+    @pl.when(at_end)
+    def _():
+        gate_to(nears[0])
 
     locals_[0].wait()
     q_own.wait()
@@ -467,12 +479,11 @@
         for piece in range(ranks):
             slot = qb.at[0, piece]
             send(slot, qb.at[1, piece], qz_s, qz_r.at[piece], (at_part(inward), core))
-        for target in nears:
-            gate_to(target)
+        gate_to(nears[1])
+        gate_to(nears[2])
         down_to(nears[0])
         gu_pass(nears[0])
         gu_halves(part)
-        dn_halves(part)
         gu_halves(nears[0])
         dn_pass(nears[0])
         gu_pass(second)
@@ -481,14 +492,9 @@
     def _():
         kv_hop(0)
         gate_to(nears[2])
-        gate_to(nears[1])
-        down_to(nears[2])
-        down_to(nears[1])
         gu_halves(part)
         dn_halves(part)
         kv_hop(1)
-        for piece in range(ranks):
-            landed(qb.at[1, piece], qz_s, qz_r.at[piece])
         def attend_near(turn_by):
             piece = (rank + turn_by) % ranks
             attend(0, piece, asend.at[0, piece])
@@ -500,21 +506,26 @@
                 (part * ranks + piece, core),
             )
 
+        gu_pass(nears[0])
 
         @pl.loop(1, 4)
         def _(turn_by):
             attend_near(turn_by)
 
-        gu_pass(nears[0])
+        gate_to(nears[1])
+        for piece in range(ranks):
+            landed(qb.at[1, piece], qz_s, qz_r.at[piece])
 
         @pl.loop(0, 3)
         def _(piece):
             attend_away(piece)
 
+        gu_halves(nears[0])
         gu_pass(second)
+        down_to(nears[2])
+        down_to(nears[1])
         attend_away(3)
         attend(0, rank, ab.at[rank])
-        gu_halves(nears[0])
 
     loads[2].wait()
     for e in flips:
@@ -580,6 +591,7 @@
         tail = jnp.where(where < half_lane, rest / (1.0 + jnp.exp(-rest)) * turned, 0.0)
         hb[source, :, main : main + 128] = tail.astype(jnp.bfloat16)
 
+    edge = jnp.where(inner, nears[0], part)
     order = nears + (part,)
     wide_cols = ranks * cols
     first_cols, later_cols = (1, 2), (0, 3)
@@ -619,11 +631,6 @@
 
     gu_halves(second)
     gu_pass(third)
-
-    @pl.when(inner)
-    def _():
-        dn_pass(nears[0])
-
     hop(0, outer)
 
     @pl.when(at_end)
@@ -632,8 +639,17 @@
         down_to(nears[2])
 
     gu_halves(third)
-    dn_halves(nears[0])
     dn_pass(nears[1])
+
+    @pl.when(at_end)
+    def _():
+        dn_halves(nears[0])
+        own_downs()
+
+    @pl.when(inner)
+    def _():
+        dn_pass(nears[0])
+
     gu_own.wait()
     landed(gu_at(0, 0, ranks * depth), gh_s, gh_r)
     feed(nears[0])
@@ -641,16 +657,16 @@
     feed(part)
     dn_halves(nears[1])
     locals_[1].wait()
-    dn_done(part)
-    dn_done(nears[0])
+    dn_done(jnp.where(inner, part, nears[0]))
     dn_done(nears[1])
     stage(first_cols, 0)
     stage(first_cols, 3)
     ends_on(first_cols, 0)
     hop(1)
+    dn_halves(edge)
+    dn_pass(nears[2])
     feed(nears[1])
     stage(first_cols, 1)
-    dn_pass(nears[2])
     ends_on(first_cols, 1)
     hop(2)
     feed(nears[2])
@@ -662,18 +678,19 @@
     def _():
         onward(first_cols, 1, False)
 
+    dn_done(edge)
     dn_done(nears[2])
+    stage(later_cols, 2)
+    stage(later_cols, 1)
+    ends_on(later_cols, 2)
     stage(later_cols, 0)
-    stage(later_cols, 1)
-    ends_on(later_cols, 0)
-    stage(later_cols, 2)
     ends_on(later_cols, 1)
     stage(later_cols, 3)
-    ends_on(later_cols, 2)
+    ends_on(later_cols, 0)
 
     @pl.when(inner)
     def _():
-        for blocks, place in ((first_cols, 2), (first_cols, 0), (later_cols, 1), (later_cols, 2), (later_cols, 0)):
+        for blocks, place in ((first_cols, 2), (first_cols, 0), (later_cols, 2), (later_cols, 0), (later_cols, 1)):
             onward(blocks, place, False)
 
     for b in first_cols + later_cols:

time: 136 us -> 127 us (0.934)
  Pallas kernels: 134 us -> 125 us
    pallas_call x1, Pallas kernels: 134 us -> 125 us  [run_layer(): pl.pallas_call(functools.partial(layer_kernel, ranks, head_dim), out_shap...]
where the time goes in v3:
time: 127 us
  Pallas kernels  125 us (98%)
  local copies, waits for them, and re-layouts  1.77 us (1%)
    pallas_call x1, Pallas kernels, run_layer(): pl.pallas_call(functools.partial(layer_kernel, ranks, head_dim), out_shap...  125 us

profile of v3, /device:TPU:0, one launch (start us, length us, event | category | flops | bytes accessed | tf_op | source)
XLA Modules:
  0.0 126.7 jit_solution(1206584713672288798)
XLA Ops:
  0.0 124.9 %shard_map.118 = bf16[96,2048]{1,0:T(8,128)(2,1)} custom-call(bf16[192,512]{1,0:T(8,128)(2,1)} %key_ref.1, bf16[192,512]{1,0:T(8,128)(2,1)} %value_ref.1, bf16[192,1024]{1,0:T(8,128)(2,1)} %query_ref.1, f32[1,128]{1,0:T(1,128)} %bitcast.4, f32[1,128]{1,0:T(1,128)} %bitcast.5, f32[1,128]{1,0:T(1,128)} %constant.3.freq_ref, bf16[128,2816]{1,0:T(8,128)(2,1)} %gate_hbm.1, ...), custom_call_target="tpu_custom_call" | custom-call | tf_op jit(solution)/shard_map/pallas_call | solution.py:781
  124.9 1.8 %copy.14 = bf16[96,2048]{1,0:T(8,128)(2,1)} copy(bf16[96,2048]{1,0:T(8,128)(2,1)} %shard_map.118) | data formatting | bytes 786432

commit v4 on v3

--- a/solution.py
+++ b/solution.py
@@ -549,15 +549,21 @@
     level = lax.rsqrt(jnp.mean(wide * wide, axis=-1, keepdims=True) + EPSILON)
     nb[part, core] = (wide * level * gain_ref[...]).astype(jnp.bfloat16)
 
-    def step_on(source, step, way):
-        slot = nb.at[source, core]
+    half_rows = share // 2
+
+    def rows_of(source, piece):
+        return nb.at[source, core, pl.ds(piece * half_rows, half_rows)]
+
+    def step_on(source, step, way, piece):
+        slot = rows_of(source, piece)
 
         @pl.when(ways[way][0])
         def _():
-            send(slot, slot, nz_s.at[way, step], nz_r.at[way, step], (sp + ranks * ways[way][1], core))
-
-    step_on(part, 0, 0)
-    step_on(part, 0, 1)
+            send(slot, slot, nz_s.at[way, step, piece], nz_r.at[way, step, piece], (sp + ranks * ways[way][1], core))
+
+    for piece in (0, 1):
+        step_on(part, 0, 0, piece)
+        step_on(part, 0, 1, piece)
     mine = nb.at[part, core]
     send(mine, mine, np_s, np_r.at[part], (sp, other))
 
@@ -567,10 +573,11 @@
 
             @pl.when(there & chosen[way])
             def _():
+                for piece in (0, 1):
+                    landed(rows_of(source, piece), nz_s.at[way, step, piece], nz_r.at[way, step, piece])
+                    if step < SPLIT - 2:
+                        step_on(source, step + 1, way, piece)
                 slot = nb.at[source, core]
-                landed(slot, nz_s.at[way, step], nz_r.at[way, step])
-                if step < SPLIT - 2:
-                    step_on(source, step + 1, way)
                 send(slot, slot, np_s, np_r.at[source], (sp, other))
 
     outer = (at_end | (high == 0), at_end | (high == 1))
@@ -594,40 +601,50 @@
     edge = jnp.where(inner, nears[0], part)
     order = nears + (part,)
     wide_cols = ranks * cols
-    first_cols, later_cols = (1, 2), (0, 3)
+    planes = (jnp.where(inner, part, nears[0]), edge, nears[1], nears[2])
+
+    def lanes_of(b):
+        return pl.ds(pl.multiple_of(b * wide_cols, wide_cols), wide_cols)
 
     def pair_sum(b, place):
         landed(drv.at[b, place], dp_s, dp_r.at[b, place])
         return dsb[b, order[place], core].astype(jnp.float32) + drv[b, place].astype(jnp.float32)
 
-    def onward(blocks, place, first):
+    def onward(k, place, first):
+        b = planes[k]
         target = order[place]
         way = 1 - (target > part).astype(jnp.int32)
-        for b in blocks:
-            total = pair_sum(b, place)
-            if not first:
-                landed(dzb.at[b, way, target], fz_s, fz_r.at[b, way, target])
-                total = total + dzb[b, way, target].astype(jnp.float32)
-            ds2[b, target] = total.astype(jnp.bfloat16)
-            send(
-                ds2.at[b, target],
-                dzb.at[b, way, target],
-                fz_s,
-                fz_r.at[b, way, target],
-                (sp + ranks * (1 - 2 * way), core),
-            )
-
-    def stage(blocks, place):
+        total = pair_sum(b, place)
+        if not first:
+            landed(dzb.at[b, way, target], fz_s, fz_r.at[b, way, target])
+            total = total + dzb[b, way, target].astype(jnp.float32)
+        ds2[b, target] = total.astype(jnp.bfloat16)
+        send(
+            ds2.at[b, target],
+            dzb.at[b, way, target],
+            fz_s,
+            fz_r.at[b, way, target],
+            (sp + ranks * (1 - 2 * way), core),
+        )
+
+    def stage(k, place):
+        b = planes[k]
         target = order[place]
-        for b in blocks:
-            block = jnp.dot(hb[target], wdn[:, b * wide_cols : (b + 1) * wide_cols], preferred_element_type=jnp.float32)
-            dsb[b, target] = block.astype(jnp.bfloat16).reshape(2, share, wide_cols)
-            send(dsb.at[b, target, other], drv.at[b, place], dp_s, dp_r.at[b, place], (sp, other))
-
-    def ends_on(blocks, place):
+        block = jnp.dot(hb[target], wdn[:, lanes_of(b)], preferred_element_type=jnp.float32)
+        dsb[b, target] = block.astype(jnp.bfloat16).reshape(2, share, wide_cols)
+        send(dsb.at[b, target, other], drv.at[b, place], dp_s, dp_r.at[b, place], (sp, other))
+
+    def ends_on(*steps):
         @pl.when(at_end)
         def _():
-            onward(blocks, place, True)
+            for k, place in steps:
+                onward(k, place, True)
+
+    def inner_on(*steps):
+        @pl.when(inner)
+        def _():
+            for k, place in steps:
+                onward(k, place, False)
 
     gu_halves(second)
     gu_pass(third)
@@ -639,12 +656,12 @@
         down_to(nears[2])
 
     gu_halves(third)
+
+    @pl.when(at_end)
+    def _():
+        dn_halves(nears[0])
+
     dn_pass(nears[1])
-
-    @pl.when(at_end)
-    def _():
-        dn_halves(nears[0])
-        own_downs()
 
     @pl.when(inner)
     def _():
@@ -653,48 +670,56 @@
     gu_own.wait()
     landed(gu_at(0, 0, ranks * depth), gh_s, gh_r)
     feed(nears[0])
+    locals_[1].wait()
+    dn_done(planes[0])
+    stage(0, 0)
     hop(0, across)
     feed(part)
     dn_halves(nears[1])
-    locals_[1].wait()
-    dn_done(jnp.where(inner, part, nears[0]))
-    dn_done(nears[1])
-    stage(first_cols, 0)
-    stage(first_cols, 3)
-    ends_on(first_cols, 0)
+
+    @pl.when(at_end)
+    def _():
+        own_downs()
+        onward(0, 0, True)
+
     hop(1)
-    dn_halves(edge)
     dn_pass(nears[2])
     feed(nears[1])
-    stage(first_cols, 1)
-    ends_on(first_cols, 1)
+    stage(0, 1)
+    dn_halves(edge)
+    dn_done(nears[1])
+    stage(2, 0)
+    ends_on((0, 1),)
+    stage(2, 1)
+    ends_on((2, 0), (2, 1))
+    dn_halves(nears[2])
     hop(2)
     feed(nears[2])
-    stage(first_cols, 2)
-    dn_halves(nears[2])
-    ends_on(first_cols, 2)
-
-    @pl.when(inner)
-    def _():
-        onward(first_cols, 1, False)
-
+    stage(0, 2)
+    stage(2, 2)
     dn_done(edge)
+    ends_on((0, 2), (2, 2))
+    stage(1, 2)
+    stage(1, 1)
+    ends_on((1, 2),)
+    stage(1, 0)
+    inner_on((0, 1), (2, 1))
     dn_done(nears[2])
-    stage(later_cols, 2)
-    stage(later_cols, 1)
-    ends_on(later_cols, 2)
-    stage(later_cols, 0)
-    ends_on(later_cols, 1)
-    stage(later_cols, 3)
-    ends_on(later_cols, 0)
-
-    @pl.when(inner)
-    def _():
-        for blocks, place in ((first_cols, 2), (first_cols, 0), (later_cols, 2), (later_cols, 0), (later_cols, 1)):
-            onward(blocks, place, False)
-
-    for b in first_cols + later_cols:
-        lanes = slice(b * wide_cols, (b + 1) * wide_cols)
+    stage(3, 2)
+    stage(3, 1)
+    ends_on((3, 2),)
+    stage(3, 0)
+    ends_on((1, 1), (3, 1))
+    stage(0, 3)
+    ends_on((1, 0), (3, 0))
+    stage(1, 3)
+    stage(2, 3)
+    stage(3, 3)
+    inner_on((0, 2), (2, 2), (2, 0), (0, 0), (1, 2), (3, 2), (3, 0), (1, 0), (1, 1), (3, 1))
+
+    for k in (2, 0, 3, 1):
+        b = planes[k]
+        lanes = lanes_of(b)
         acc = pair_sum(b, last)
         base = st[:, lanes].astype(jnp.float32)
 
@@ -714,7 +739,7 @@
         def _():
             out_ref[:, lanes] = (base + 0.5 * add(1, add(0, acc))).astype(jnp.bfloat16)
 
-        pltpu.make_async_copy(out_ref.at[:, lanes], out_hbm.at[:, lanes], local_sem.at[7 + b]).start()
+        pltpu.make_async_copy(out_ref.at[:, lanes], out_hbm.at[:, lanes], local_sem.at[7 + k]).start()
 
     left(kv_ref.at[pl.ds(0, last)], kvp_s, kvp_r.at[1])
     left(q_ref.at[pl.ds(0, last)], q_s, q_r.at[1])
@@ -734,7 +759,8 @@
 
             @pl.when(ways[way][0] & there)
             def _():
-                left(nb.at[source, core], nz_s.at[way, step], nz_r.at[way, step])
+                for piece in (0, 1):
+                    left(rows_of(source, piece), nz_s.at[way, step, piece], nz_r.at[way, step, piece])
 
             if step < 2:
 
@@ -754,9 +780,9 @@
         for e in flips:
             left(asend.at[0, flip(e)], at_s.at[0, flip(e)], at_r.at[rank])
 
-    for b in range(SPLIT):
-        lanes = slice(b * wide_cols, (b + 1) * wide_cols)
-        pltpu.make_async_copy(out_ref.at[:, lanes], out_hbm.at[:, lanes], local_sem.at[7 + b]).wait()
+    for k in range(SPLIT):
+        lanes = lanes_of(planes[k])
+        pltpu.make_async_copy(out_ref.at[:, lanes], out_hbm.at[:, lanes], local_sem.at[7 + k]).wait()
 
 
 def run_layer(key, value, query, k_gain, q_gain, gate, up, down, out_weight, resid, gain, ranks):
@@ -813,7 +839,7 @@
         + [dma((SPLIT, 2))] * 2
         + [dma((SPLIT, SPLIT)), dma((2, SPLIT))]
         + [dma((2, 2, ranks))] * 2
-        + [dma((2, SPLIT - 1))] * 2
+        + [dma((2, SPLIT - 1, 2))] * 2
         + [dma((SPLIT, 2, SPLIT))],
         compiler_params=pltpu.CompilerParams(
             collective_id=0, has_side_effects=True, vmem_limit_bytes=62 * 1024 * 1024

time: 127 us -> 125 us (0.984)
  Pallas kernels: 125 us -> 122 us
    pallas_call x1, Pallas kernels: 125 us -> 122 us  [run_layer(): pl.pallas_call(functools.partial(layer_kernel, ranks, head_dim), out_shap...]
where the time goes in v4:
time: 125 us; the launch traced here: 124 us
  Pallas kernels  122 us (98%)
  local copies, waits for them, and re-layouts  1.77 us (1%)
    pallas_call x1, Pallas kernels, run_layer(): pl.pallas_call(functools.partial(layer_kernel, ranks, head_dim), out_shap...  122 us

profile of v4, /device:TPU:0, one launch (start us, length us, event | category | flops | bytes accessed | tf_op | source)
XLA Modules:
  0.0 124.2 jit_solution(3609102024847620669)
XLA Ops:
  0.0 122.5 %shard_map.118 = bf16[96,2048]{1,0:T(8,128)(2,1)} custom-call(bf16[192,512]{1,0:T(8,128)(2,1)} %key_ref.1, bf16[192,512]{1,0:T(8,128)(2,1)} %value_ref.1, bf16[192,1024]{1,0:T(8,128)(2,1)} %query_ref.1, f32[1,128]{1,0:T(1,128)} %bitcast.4, f32[1,128]{1,0:T(1,128)} %bitcast.5, f32[1,128]{1,0:T(1,128)} %constant.3.freq_ref, bf16[128,2816]{1,0:T(8,128)(2,1)} %gate_hbm.1, ...), custom_call_target="tpu_custom_call" | custom-call | tf_op jit(solution)/shard_map/pallas_call | solution.py:807
  122.5 1.8 %copy.14 = bf16[96,2048]{1,0:T(8,128)(2,1)} copy(bf16[96,2048]{1,0:T(8,128)(2,1)} %shard_map.118) | data formatting | bytes 786432

commit v5 on v4

--- a/solution.py
+++ b/solution.py
@@ -715,7 +715,7 @@
     stage(1, 3)
     stage(2, 3)
     stage(3, 3)
-    inner_on((0, 2), (2, 2), (2, 0), (0, 0), (1, 2), (3, 2), (3, 0), (1, 0), (1, 1), (3, 1))
+    inner_on((0, 2), (2, 2), (1, 2), (2, 0), (3, 2), (0, 0), (1, 1), (3, 0), (3, 1), (1, 0))
 
     for k in (2, 0, 3, 1):
         b = planes[k]

time: 125 us -> 123 us (0.984)
  no operation moved by 1% of the time
where the time goes in v5:
time: 123 us
  Pallas kernels  121 us (98%)
  local copies, waits for them, and re-layouts  1.77 us (1%)
    pallas_call x1, Pallas kernels, run_layer(): pl.pallas_call(functools.partial(layer_kernel, ranks, head_dim), out_shap...  121 us

profile of v5, /device:TPU:0, one launch (start us, length us, event | category | flops | bytes accessed | tf_op | source)
XLA Modules:
  0.0 123.1 jit_solution(12047584726237818719)
XLA Ops:
  0.0 121.3 %shard_map.118 = bf16[96,2048]{1,0:T(8,128)(2,1)} custom-call(bf16[192,512]{1,0:T(8,128)(2,1)} %key_ref.1, bf16[192,512]{1,0:T(8,128)(2,1)} %value_ref.1, bf16[192,1024]{1,0:T(8,128)(2,1)} %query_ref.1, f32[1,128]{1,0:T(1,128)} %bitcast.4, f32[1,128]{1,0:T(1,128)} %bitcast.5, f32[1,128]{1,0:T(1,128)} %constant.3.freq_ref, bf16[128,2816]{1,0:T(8,128)(2,1)} %gate_hbm.1, ...), custom_call_target="tpu_custom_call" | custom-call | tf_op jit(solution)/shard_map/pallas_call | solution.py:807
  121.3 1.8 %copy.14 = bf16[96,2048]{1,0:T(8,128)(2,1)} copy(bf16[96,2048]{1,0:T(8,128)(2,1)} %shard_map.118) | data formatting | bytes 786432
